TPU v7x, 32 devices: a whole 2x2x4 slice. The times are simulated.
32 devices in a mesh: fs: 16 (over z, y, x), tp: 2 (over core).
Axes of the slice: x: 2, y: 2, z: 4, core: 2. Of those that a mesh axis runs over, the one named last changes fastest.
Arguments:
- tokens: bfloat16 [8192, 2048], P('fs'), may hold values from -6 to 6
- mixer_gain: float32 [2048], replicated, may hold values from 0.1 to 1.9
- w_query: bfloat16 [2048, 1024], P('fs', 'tp'), may hold values from -0.125 to 0.125
- w_key: bfloat16 [2048, 1024], P('fs', 'tp'), may hold values from -0.125 to 0.125
- w_value: bfloat16 [2048, 2048], P('fs', 'tp'), may hold values from -0.125 to 0.125
- gate_down: bfloat16 [2048, 32], replicated, may hold values from -0.125 to 0.125
- gate_up: bfloat16 [32, 1024], P(None, 'tp'), may hold values from -1 to 1
- decay_bias: float32 [1024], P('tp'), may hold values from -1 to 6
- decay_shift: float32 [8192, 8], P('fs', 'tp'), may hold values from -0.71 to 0, as said below
- head_gain: float32 [2048], P('tp'), may hold values from 0.1 to 1.9
- w_out: bfloat16 [2048, 2048], P('fs', 'tp'), may hold values from -0.125 to 0.125
- mlp_gain: float32 [2048], replicated, may hold values from 0.1 to 1.9
- mlp_up: bfloat16 [2048, 8192], P('fs', 'tp'), may hold values from -0.125 to 0.125
- mlp_down: bfloat16 [2048, 8192], P('fs', 'tp'), may hold values from -0.0625 to 0.0625
Outputs:
- layer_out: bfloat16 [8192, 2048], P('fs')
Inputs may be any that keep to these rules, and one draw needn't show every extreme that they name: `decay_shift`: never positive.
All inputs are finite; a program needn't handle non-finite values.
Results may differ from a plain program's by a relative error of at most 0.022.
Values may be sent and summed in bfloat16 or wider, within the bound.
A program may use at most 128 MiB of HBM per device.

v0:
```python
import jax
import jax.numpy as jnp
from jax import lax
from jax.sharding import PartitionSpec as P

BLOCK_TOKENS = 64


epsilon = 1e-06
decay_temper = 16.0
highest = lax.Precision.HIGHEST


def rms_rows(row_block, row_gain):
    values = row_block.astype(jnp.float32)
    inverse = lax.rsqrt(jnp.mean(values * values, axis=-1, keepdims=True) + epsilon)
    return (values * inverse * row_gain).astype(jnp.bfloat16)


def mix_heads(queries, keyed, valued, gate_low, gate_up, decay_bias, seq_shift, head_gain):
    length = queries.shape[0]
    head_count = seq_shift.shape[1]
    head_k = queries.shape[1] // head_count
    head_v = valued.shape[1] // head_count
    blocks = length // BLOCK_TOKENS
    half = jnp.bfloat16
    full = jnp.float32
    gate_pre = jnp.dot(gate_low, gate_up, preferred_element_type=full) + decay_bias
    log_decay = jax.nn.log_sigmoid(gate_pre) / decay_temper
    log_decay = log_decay.reshape(length, head_count, head_k) + seq_shift[:, :, None]

    def to_blocks(tensor):
        return tensor.reshape(blocks, BLOCK_TOKENS, head_count, -1).transpose(0, 2, 1, 3)

    query_b = to_blocks(queries).astype(full) * head_k ** (-0.5)
    key_b = to_blocks(keyed).astype(full)
    value_b = to_blocks(valued)
    decay_b = to_blocks(log_decay)
    lower = jnp.tril(jnp.ones((BLOCK_TOKENS, BLOCK_TOKENS), full))
    ahead = jnp.einsum("ts,nhsd->nhtd", lower, decay_b, precision=highest)
    back = jnp.einsum("st,nhsd->nhtd", lower, decay_b, precision=highest)
    end = jnp.sum(decay_b, axis=2, keepdims=True)
    q_ahead = (query_b * jnp.exp(ahead)).astype(half)
    q_back = (query_b * jnp.exp(back)).astype(half)
    k_ahead = (key_b * jnp.exp(-ahead)).astype(half)
    k_back = (key_b * jnp.exp(-back)).astype(half)
    score = "nhtd,nhsd->nhts"
    keep = lower > 0
    scores = jnp.where(
        keep, jnp.einsum(score, q_ahead, k_ahead, preferred_element_type=full), 0.0
    ) + jnp.where(keep.T, jnp.einsum(score, q_back, k_back, preferred_element_type=full), 0.0)
    within = jnp.einsum(
        "nhts,nhsv->nhtv", scores.astype(half), value_b, preferred_element_type=full
    )
    tails = jnp.concatenate(
        [key_b * jnp.exp(end - ahead), key_b * jnp.exp(end - back)], axis=-1
    ).astype(half)
    contrib = jnp.einsum("nhsd,nhsv->nhdv", tails, value_b, preferred_element_type=full)
    fading = jnp.exp(end[:, :, 0, :])[..., None]
    before = [jnp.zeros((head_count, head_k, head_v), full)]
    for block in range(blocks - 1):
        before.append(fading[block] * before[-1] + contrib[block, :, :head_k])
    after = [jnp.zeros((head_count, head_k, head_v), full)]
    for block in range(blocks - 1, 0, -1):
        after.append(fading[block] * after[-1] + contrib[block, :, head_k:])
    states = jnp.concatenate(
        [jnp.stack([s.astype(half) for s in before]),
         jnp.stack([s.astype(half) for s in after[::-1]])], axis=2
    )
    both = jnp.concatenate([q_ahead, q_back], axis=-1)
    outcome = within + jnp.einsum("nhtd,nhdv->nhtv", both, states, preferred_element_type=full)
    inverse = lax.rsqrt(jnp.mean(outcome * outcome, axis=-1, keepdims=True) + epsilon)
    normed = outcome * inverse * head_gain.reshape(head_count, 1, head_v)
    return normed.astype(half).transpose(0, 2, 1, 3).reshape(length, head_count * head_v)


def times_transposed(left, weight_rows):
    return lax.dot_general(
        left, weight_rows, (((1,), (1,)), ((), ())), preferred_element_type=jnp.float32
    )


def per_device(
    tokens,
    mixer_gain,
    w_query,
    w_key,
    w_value,
    gate_down,
    gate_up,
    decay_bias,
    decay_shift,
    head_gain,
    w_out,
    mlp_gain,
    mlp_up,
    mlp_down,
):
    rows_all = rms_rows(tokens, mixer_gain)
    gate_low = jnp.dot(rows_all, gate_down, preferred_element_type=jnp.float32).astype(jnp.bfloat16)
    joined = jnp.concatenate([w_query, w_key, w_value], axis=1)
    joined = lax.all_gather(joined, "fs", axis=0, tiled=True)
    sums = jnp.dot(rows_all, joined, preferred_element_type=jnp.float32).astype(jnp.bfloat16)
    wide = w_query.shape[1]
    query_sum, key_sum, value_sum = jnp.split(sums, (wide, 2 * wide), axis=1)
    mixer_out = mix_heads(
        query_sum,
        key_sum,
        value_sum,
        gate_low,
        gate_up,
        decay_bias,
        decay_shift,
        head_gain,
    )
    out_all = lax.all_gather(w_out, "fs", axis=0, tiled=True)
    mixer_term = times_transposed(mixer_out, out_all).astype(jnp.bfloat16).astype(jnp.float32)
    mixer_sum = lax.psum(mixer_term.astype(jnp.bfloat16), "tp").astype(jnp.float32)
    after_mixer = (tokens.astype(jnp.float32) + mixer_sum).astype(jnp.bfloat16)
    rows_two = rms_rows(after_mixer, mlp_gain)
    up_all, down_all = (
        lax.all_gather(mlp_up, "fs", axis=0, tiled=True),
        lax.all_gather(mlp_down, "fs", axis=0, tiled=True),
    )
    hidden = jnp.square(
        jax.nn.relu(jnp.dot(rows_two, up_all, preferred_element_type=jnp.float32))
    ).astype(jnp.bfloat16)
    mlp_term = times_transposed(hidden, down_all).astype(jnp.bfloat16).astype(jnp.float32)
    mlp_total = lax.psum(mlp_term.astype(jnp.bfloat16), "tp").astype(jnp.float32)
    return (after_mixer.astype(jnp.float32) + mlp_total).astype(jnp.bfloat16)


def solution(mesh):
    return jax.shard_map(
        per_device,
        mesh=mesh,
        in_specs=(
            P("fs", None),
            P(),
            P("fs", "tp"),
            P("fs", "tp"),
            P("fs", "tp"),
            P(),
            P(None, "tp"),
            P("tp"),
            P("fs", "tp"),
            P("tp"),
            P("fs", "tp"),
            P(),
            P("fs", "tp"),
            P("fs", "tp"),
        ),
        out_specs=P("fs", None),
        check_vma=False,
    )
```

profile of v0, /device:TPU:0, one launch (start us, length us, event | category | flops | bytes accessed | tf_op | source)
XLA Modules:
  0.0 669.9 jit_solution(15815060779051155320)
XLA Ops:
  6.6 2.0 pad_maximum_fusion
  8.7 0.7 all-gather.7.cloned.1.call-update
  9.5 2.1 fusion
  11.6 2.5 fusion.25
  14.1 1.6 reshape.78
  15.8 0.4 bitcast_reduce_fusion
  16.2 0.1 copy.29
  16.3 0.1 copy.23
  16.5 0.7 broadcast_dynamic-update-slice_fusion.1
  17.2 2.3 fusion.41
  19.5 105.7 %all-gather.5.cloned.1.call-done = bf16[2048,2048]{1,0:T(8,128)(2,1)} async-done(((bf16[128,2048]{1,0:T(8,128)(2,1)}), bf16[2048,2048]{1,0:T(8,128)(2,1)}) %all-gather.5.cloned.1.call-update) | async-done | bytes 8388624 | tf_op jit(solution)/shard_map/all_gather | solution.py:102
  125.2 8.2 %convolution_convert_fusion.1 = bf16[512,2048]{1,0:T(8,128)(2,1)S(1)} fusion(bf16[2048,2048]{1,0:T(8,128)(2,1)} %all-gather.5.cloned.1.call-done, bf16[512,2048]{1,0:T(8,128)(2,1)S(1)} %copy-done.2, f32[2048]{0:T(1024)S(1)} %copy-done.12, f32[512]{0:T(512)S(1)} %add_rsqrt_fusion.1), kind=kOutput, calls=%fused_computation.21 | convolution fusion | flops 4300210176 | bytes 12593152 | tf_op jit(solution)/shard_map/dot_general | solution.py:103
  133.5 1.2 split.14
  134.6 0.5 copy-done.7
  135.1 1.1 slice_convert_fusion
  136.2 1.6 reshape.81
  137.8 2.2 convert_multiply_fusion.4
  140.0 2.5 mul.260
  142.5 2.6 reshape.79
  145.1 4.7 fusion.34
  149.9 1.3 fusion.29
  151.2 0.5 copy-done.8
  151.6 0.1 fusion.62
  151.8 0.2 convert_dynamic-update-slice_fusion.9
  152.0 0.1 convert_dynamic-update-slice_fusion.8
  152.1 0.2 convert_dynamic-update-slice_fusion.7
  152.4 0.1 convert_dynamic-update-slice_fusion.6
  152.5 0.9 convert_dynamic-update-slice_fusion.5
  153.4 0.1 convert_dynamic-update-slice_fusion.3
  153.6 0.2 fusion.63
  153.9 0.1 fusion.61
  154.1 2.2 fusion.8
  156.2 1.4 convolution_select_fusion
  157.6 4.8 multiply_reduce_fusion
  162.4 2.0 fusion.16
  164.4 0.8 copy.31
  165.2 0.2 copy.35
  165.5 36.3 %all-gather.7.cloned.1.call-done = bf16[2048,1024]{1,0:T(8,128)(2,1)} async-done(((bf16[128,1024]{1,0:T(8,128)(2,1)}), bf16[2048,1024]{1,0:T(8,128)(2,1)}) %all-gather.7.cloned.1.call-update) | async-done | bytes 4194320 | tf_op jit(solution)/shard_map/all_gather | solution.py:116
  201.7 5.9 convolution_convert_fusion
  207.7 0.5 all-gather.11.cloned.1.call-update
  208.3 0.5 all-gather.9.cloned.1.call-update
  208.9 18.8 %all-reduce.3.cloned.1.call-done = bf16[512,2048]{1,0:T(8,128)(2,1)} async-done(((bf16[512,2048]{1,0:T(8,128)(2,1)}), bf16[512,2048]{1,0:T(8,128)(2,1)}) %all-reduce.3.cloned.1.call-update) | async-done | bytes 2097168 | tf_op jit(solution)/shard_map/psum | solution.py:118
  227.7 2.3 fusion.4
  230.1 192.5 %all-gather.11.cloned.1.call-done = bf16[2048,4096]{1,0:T(8,128)(2,1)} async-done(((bf16[128,4096]{1,0:T(8,128)(2,1)}), bf16[2048,4096]{1,0:T(8,128)(2,1)}) %all-gather.11.cloned.1.call-update) | async-done | bytes 16777232 | tf_op jit(solution)/shard_map/all_gather | solution.py:123
  422.5 191.8 %all-gather.9.cloned.1.call-done = bf16[2048,4096]{1,0:T(8,128)(2,1)} async-done(((bf16[128,4096]{1,0:T(8,128)(2,1)}), bf16[2048,4096]{1,0:T(8,128)(2,1)}) %all-gather.9.cloned.1.call-update) | async-done | bytes 16777232 | tf_op jit(solution)/shard_map/all_gather | solution.py:122
  614.4 24.0 %convolution_convert_fusion.2 = bf16[512,2048]{1,0:T(8,128)(2,1)} fusion(bf16[2048,4096]{1,0:T(8,128)(2,1)} %all-gather.11.cloned.1.call-done, bf16[2048,4096]{1,0:T(8,128)(2,1)} %all-gather.9.cloned.1.call-done, f32[2048]{0:T(1024)S(1)} %copy-done.13, f32[512]{0:T(512)S(1)} %add_rsqrt_fusion, bf16[512,2048]{1,0:T(8,128)(2,1)S(1)} %copy-done.2, ...), kind=kOutput, calls=%fused_computation.22 | convolution fusion | flops 17195597824 | bytes 39856128 | tf_op jit(solution)/shard_map/dot_general | solution.py:78
  638.4 19.6 %all-reduce.5.cloned.1.call-done = bf16[512,2048]{1,0:T(8,128)(2,1)} async-done(((bf16[512,2048]{1,0:T(8,128)(2,1)}), bf16[512,2048]{1,0:T(8,128)(2,1)}) %all-reduce.5.cloned.1.call-update) | async-done | bytes 2097168 | tf_op jit(solution)/shard_map/psum | solution.py:129
  658.0 5.0 fusion.7
  (51 shorter events, 0.6 us)
Async XLA Ops:
  6.5 5.0 copy-start
  6.5 5.0 copy-start.2
  6.5 5.0 copy-start.12
  6.5 5.1 copy-start.11
  6.5 5.1 copy-start.14
  6.5 118.6 %all-gather.5.cloned.1.call-start = ((), (), s32[]{:S(2)}) async-start(), calls=%async_computation | async-start | bytes 8912896 | tf_op jit(solution)/shard_map/all_gather | solution.py:102
  8.7 193.1 %all-gather.7.cloned.1.call-start = ((), (), s32[]{:S(2)}) async-start(), calls=%async_computation.1 | async-start | bytes 4456448 | tf_op jit(solution)/shard_map/all_gather | solution.py:116
  9.4 218.3 %all-reduce.3.cloned.1.call-start = ((), (), s32[]{:S(2)}) async-start(), calls=%async_computation.2 | async-start | bytes 4194304 | tf_op jit(solution)/shard_map/psum | solution.py:118
  14.1 1.6 copy-start.9
  14.1 2.3 copy-start.10
  15.7 117.7 %copy-start.3 = (f32[8,64,4,128]{3,2,1,0:T(4,128)}, f32[8,64,4,128]{3,2,1,0:T(4,128)S(1)}, u32[]{:S(2)}) copy-start(f32[8,64,4,128]{3,2,1,0:T(4,128)S(1)} %reshape.78) | copy-start | bytes 3145732
  133.4 1.7 copy-start.7
  145.1 4.7 copy-start.5
  149.9 4.2 copy-start.6
  149.9 1.8 copy-start.8
  154.1 2.2 copy-start.4
  207.6 214.9 %all-gather.11.cloned.1.call-start = ((), (), s32[]{:S(2)}) async-start(), calls=%async_computation.4 | async-start | bytes 17825792 | tf_op jit(solution)/shard_map/all_gather | solution.py:123
  208.2 406.2 %all-gather.9.cloned.1.call-start = ((), (), s32[]{:S(2)}) async-start(), calls=%async_computation.3 | async-start | bytes 17825792 | tf_op jit(solution)/shard_map/all_gather | solution.py:122
  208.8 405.6 %copy-start.13 = (f32[2048]{0:T(1024)S(1)}, f32[2048]{0:T(1024)}, u32[]{:S(2)}) copy-start(f32[2048]{0:T(1024)} %param.25) | copy-start | bytes 24580
  208.8 449.2 %all-reduce.5.cloned.1.call-start = ((), (), s32[]{:S(2)}) async-start(), calls=%async_computation.5 | async-start | bytes 4194304 | tf_op jit(solution)/shard_map/psum | solution.py:129
  658.0 5.0 copy-start.1
Sparse Core Ops, SparseCore 0:
  10.1 115.0 all-gather.4
  127.9 73.7 all-gather.6
  207.8 19.8 all-reduce.2
  230.3 192.1 all-gather.10
  425.2 189.1 all-gather.8
  638.5 19.4 all-reduce.4
where the time goes:
time: 670 us
  waiting for transfers between devices  567 us (85%)
  matrix products  57.2 us (9%)
  other arithmetic  19.4 us (3%)
  between operations  13.8 us (2%)
  local copies, waits for them, and re-layouts  12.6 us (2%)
    all_gather x1, waiting for transfers between devices, per_device(): lax.all_gather(mlp_down, 'fs', axis=0, tiled=True)  192 us
    all_gather x1, waiting for transfers between devices, per_device(): lax.all_gather(mlp_up, 'fs', axis=0, tiled=True)  192 us
    all_gather x1, waiting for transfers between devices, per_device(): joined = lax.all_gather(joined, 'fs', axis=0, tiled=True)  106 us
    all_gather x1, waiting for transfers between devices, per_device(): out_all = lax.all_gather(w_out, 'fs', axis=0, tiled=True)  36.3 us
    dot_general x2, matrix products, times_transposed(): lax.dot_general(left, weight_rows, (((1,), (1,)), ((), ())), preferred_el...  29.9 us
    psum x1, waiting for transfers between devices, per_device(): lax.psum(mlp_term.astype(jnp.bfloat16), 'tp').astype(jnp.float32)  19.6 us
    psum x1, waiting for transfers between devices, per_device(): lax.psum(mixer_term.astype(jnp.bfloat16), 'tp').astype(jnp.float32)  18.8 us
  transfers between devices with their start and end apart: 6, of which 6 were waited for; matrix products, arithmetic and copies ran while one was open for 8% of the time, Pallas kernels for 0%

commit v1 on v0

--- a/solution.py
+++ b/solution.py
@@ -1,9 +1,14 @@
+import functools
+
 import jax
 import jax.numpy as jnp
 from jax import lax
-from jax.sharding import PartitionSpec as P
+from jax.experimental import pallas as pl
+from jax.experimental.pallas import tpu as pltpu
+from jax.sharding import Mesh, PartitionSpec as P
 
 BLOCK_TOKENS = 64
+SHARE = 4
 
 
 epsilon = 1e-06
@@ -17,20 +22,25 @@
     return (values * inverse * row_gain).astype(jnp.bfloat16)
 
 
-def mix_heads(queries, keyed, valued, gate_low, gate_up, decay_bias, seq_shift, head_gain):
-    length = queries.shape[0]
+def mix_heads(
+    queries, keyed, valued, gate_low, gate_up, decay_bias, seq_shift, head_gain, sequences
+):
+    rows = queries.shape[0]
     head_count = seq_shift.shape[1]
     head_k = queries.shape[1] // head_count
     head_v = valued.shape[1] // head_count
-    blocks = length // BLOCK_TOKENS
+    blocks = rows // sequences // BLOCK_TOKENS
+    lanes = sequences * head_count
     half = jnp.bfloat16
     full = jnp.float32
     gate_pre = jnp.dot(gate_low, gate_up, preferred_element_type=full) + decay_bias
     log_decay = jax.nn.log_sigmoid(gate_pre) / decay_temper
-    log_decay = log_decay.reshape(length, head_count, head_k) + seq_shift[:, :, None]
+    log_decay = log_decay.reshape(rows, head_count, head_k) + seq_shift[:, :, None]
 
     def to_blocks(tensor):
-        return tensor.reshape(blocks, BLOCK_TOKENS, head_count, -1).transpose(0, 2, 1, 3)
+        wide = tensor.reshape(sequences, blocks, BLOCK_TOKENS, head_count, -1)
+        wide = wide.transpose(1, 0, 3, 2, 4)
+        return wide.reshape(blocks, lanes, BLOCK_TOKENS, -1)
 
     query_b = to_blocks(queries).astype(full) * head_k ** (-0.5)
     key_b = to_blocks(keyed).astype(full)
@@ -57,10 +67,10 @@
     ).astype(half)
     contrib = jnp.einsum("nhsd,nhsv->nhdv", tails, value_b, preferred_element_type=full)
     fading = jnp.exp(end[:, :, 0, :])[..., None]
-    before = [jnp.zeros((head_count, head_k, head_v), full)]
+    before = [jnp.zeros((lanes, head_k, head_v), full)]
     for block in range(blocks - 1):
         before.append(fading[block] * before[-1] + contrib[block, :, :head_k])
-    after = [jnp.zeros((head_count, head_k, head_v), full)]
+    after = [jnp.zeros((lanes, head_k, head_v), full)]
     for block in range(blocks - 1, 0, -1):
         after.append(fading[block] * after[-1] + contrib[block, :, head_k:])
     states = jnp.concatenate(
@@ -70,13 +80,482 @@
     both = jnp.concatenate([q_ahead, q_back], axis=-1)
     outcome = within + jnp.einsum("nhtd,nhdv->nhtv", both, states, preferred_element_type=full)
     inverse = lax.rsqrt(jnp.mean(outcome * outcome, axis=-1, keepdims=True) + epsilon)
-    normed = outcome * inverse * head_gain.reshape(head_count, 1, head_v)
-    return normed.astype(half).transpose(0, 2, 1, 3).reshape(length, head_count * head_v)
+    outcome = (outcome * inverse).reshape(blocks, sequences, head_count, BLOCK_TOKENS, head_v)
+    normed = outcome * head_gain.reshape(head_count, 1, head_v)
+    normed = normed.astype(half).transpose(1, 0, 3, 2, 4)
+    return normed.reshape(rows, head_count * head_v)
 
 
 def times_transposed(left, weight_rows):
     return lax.dot_general(
         left, weight_rows, (((1,), (1,)), ((), ())), preferred_element_type=jnp.float32
+    )
+
+
+half = jnp.bfloat16
+full = jnp.float32
+MESH = pl.DeviceIdType.MESH
+VMEM = pl.BlockSpec(memory_space=pltpu.VMEM)
+ROW_TILE = 64
+COLUMN_TILE = 256
+
+
+def flip(place, offset):
+    bit = 1
+    while bit <= offset:
+        if offset & bit:
+            place = place + bit - 2 * bit * lax.rem(lax.div(place, bit), 2)
+        bit *= 2
+    return place
+
+
+def greet(share):
+    place, core = lax.axis_index("share"), lax.axis_index("tp")
+    barrier = pltpu.get_barrier_semaphore()
+    for offset in range(1, share):
+        pl.semaphore_signal(
+            barrier, inc=1, device_id={"share": flip(place, offset)}, device_id_type=MESH
+        )
+    pl.semaphore_signal(barrier, inc=1, device_id={"tp": 1 - core}, device_id_type=MESH)
+    pl.semaphore_wait(barrier, share)
+
+
+def remote(source, target, send, receive, device):
+    return pltpu.make_async_remote_copy(
+        src_ref=source,
+        dst_ref=target,
+        send_sem=send,
+        recv_sem=receive,
+        device_id=device,
+        device_id_type=MESH,
+    )
+
+
+def block_of(index, size):
+    return pl.ds(pl.multiple_of(index * size, size), size)
+
+
+def exchange_weights(share, weights, targets, send, receive):
+    place = lax.axis_index("share")
+    copies = []
+    for number, (weight, (target, column)) in enumerate(zip(weights, targets)):
+        depth = weight.shape[0]
+        size = weight.shape[1] // share
+        rows = block_of(place, depth)
+        for offset in range(share - 1, 0, -1):
+            mate = flip(place, offset)
+            copy = remote(
+                weight.at[:, block_of(mate, size)],
+                target.at[rows, pl.ds(column, size)],
+                send.at[number, offset],
+                receive.at[number, offset],
+                {"share": mate},
+            )
+            copy.start()
+            arrival = remote(
+                weight.at[:, block_of(mate, size)],
+                target.at[block_of(mate, depth), pl.ds(column, size)],
+                send.at[number, offset],
+                receive.at[number, offset],
+                {"share": mate},
+            )
+            copies.append((copy, arrival))
+        target[rows, pl.ds(column, size)] = weight[:, block_of(place, size)]
+    return copies
+
+
+def finish(copies):
+    for copy, arrival in copies:
+        copy.wait_send()
+        arrival.wait_recv()
+
+
+def weights_kernel(share, q_ref, k_ref, v_ref, o_ref, out_ref, send, receive):
+    greet(share)
+    weights = (q_ref, k_ref, v_ref, o_ref)
+    targets, column = [], 0
+    for weight in weights:
+        targets.append((out_ref, column))
+        column += weight.shape[1] // share
+    finish(exchange_weights(share, weights, targets, send, receive))
+
+
+class Gather:
+    def __init__(self, share, part, target, plane_send, plane_receive, pair_send, pair_receive):
+        self.share, self.part, self.target = share, part, target
+        self.plane_send, self.plane_receive = plane_send, plane_receive
+        self.pair_send, self.pair_receive = pair_send, pair_receive
+        self.place, self.core = lax.axis_index("share"), lax.axis_index("tp")
+
+    def rows(self, mate, core):
+        return block_of(mate * 2 + core, self.part.shape[0])
+
+    def plane(self, offset, arriving):
+        mate = flip(self.place, offset)
+        owner = mate if arriving else self.place
+        return remote(
+            self.part,
+            self.target.at[self.rows(owner, self.core)],
+            self.plane_send.at[offset],
+            self.plane_receive.at[offset],
+            {"share": mate},
+        )
+
+    def pair(self, offset, arriving):
+        mate = flip(self.place, offset)
+        source = self.part if offset == 0 else self.target.at[self.rows(mate, self.core)]
+        return remote(
+            source,
+            self.target.at[self.rows(mate, 1 - self.core if arriving else self.core)],
+            self.pair_send.at[offset],
+            self.pair_receive.at[offset],
+            {"tp": 1 - self.core},
+        )
+
+    def start(self):
+        for offset in range(self.share - 1, 0, -1):
+            self.plane(offset, False).start()
+        self.pair(0, False).start()
+
+    def finish(self):
+        self.target[self.rows(self.place, self.core)] = self.part[...]
+        for offset in range(1, self.share):
+            self.plane(offset, True).wait_recv()
+            self.pair(offset, False).start()
+        for offset in range(self.share):
+            if offset:
+                self.plane(offset, False).wait_send()
+            self.pair(offset, False).wait_send()
+            self.pair(offset, True).wait_recv()
+
+
+def tokens_kernel(
+    share,
+    part_ref,
+    shift_ref,
+    up_ref,
+    down_ref,
+    rows_ref,
+    shifts_ref,
+    up_out,
+    down_out,
+    send,
+    receive,
+    plane_send,
+    plane_receive,
+    pair_send,
+    pair_receive,
+    shift_send,
+    shift_receive,
+):
+    greet(share)
+    place = lax.axis_index("share")
+    gather = Gather(
+        share, part_ref, rows_ref, plane_send, plane_receive, pair_send, pair_receive
+    )
+    shifts = []
+    for offset in range(1, share):
+        mate = flip(place, offset)
+        pair = [
+            remote(
+                shift_ref,
+                shifts_ref.at[owner],
+                shift_send.at[offset],
+                shift_receive.at[offset],
+                {"share": mate},
+            )
+            for owner in (place, mate)
+        ]
+        pair[0].start()
+        shifts.append(pair)
+    shifts_ref[place] = shift_ref[...]
+    copies = exchange_weights(
+        share, (up_ref, down_ref), ((up_out, 0), (down_out, 0)), send, receive
+    )
+    gather.start()
+    finish(shifts)
+    gather.finish()
+    finish(copies)
+
+
+def product_scatter(share, left_ref, weight_ref, column, base_ref, after_ref, scratch):
+    kept, to_pair, from_pair, to_plane, from_plane, sems = scratch
+    place, core = lax.axis_index("share"), lax.axis_index("tp")
+    length, width = after_ref.shape
+    wide = width // 2
+    depth = left_ref.shape[1]
+    other = 1 - core
+
+    def pair(offset):
+        return remote(
+            to_pair.at[offset], from_pair.at[offset], sems.at[0, offset], sems.at[1, offset],
+            {"tp": other},
+        )
+
+    def plane(offset):
+        return remote(
+            to_plane.at[offset], from_plane.at[offset], sems.at[2, offset], sems.at[3, offset],
+            {"share": flip(place, offset)},
+        )
+
+    def multiply(offset):
+        rows = block_of(flip(place, offset), length)
+        for columns, target in ((other, to_pair), (core, kept)):
+
+            @pl.loop(0, wide // COLUMN_TILE)
+            def _(tile):
+                start = pl.multiple_of(columns * wide + tile * COLUMN_TILE, COLUMN_TILE)
+                product = lax.dot_general(
+                    left_ref[rows, :],
+                    weight_ref[pl.ds(start, COLUMN_TILE), pl.ds(column, depth)],
+                    (((1,), (1,)), ((), ())),
+                    preferred_element_type=full,
+                )
+                target[offset, :, block_of(tile, COLUMN_TILE)] = product.astype(half)
+
+            if columns is other:
+                pair(offset).start()
+
+    def combine(offset):
+        pair(offset).wait_recv()
+
+        @pl.loop(0, length // ROW_TILE)
+        def _(tile):
+            rows = block_of(tile, ROW_TILE)
+            total = kept[offset, rows, :].astype(full) + from_pair[offset, rows, :].astype(full)
+            to_plane[offset, rows, :] = total.astype(half)
+
+        if offset:
+            plane(offset).start()
+
+    order = list(range(share - 1, -1, -1))
+    multiply(order[0])
+    for number, offset in enumerate(order):
+        if number + 1 < share:
+            multiply(order[number + 1])
+        combine(offset)
+    for offset in order[:-1]:
+        plane(offset).wait_recv()
+    mine = block_of(core, wide)
+
+    @pl.loop(0, length // ROW_TILE)
+    def _(tile):
+        rows = block_of(tile, ROW_TILE)
+        total = base_ref[rows, mine].astype(full) + to_plane[0, rows, :].astype(full)
+        for offset in range(1, share):
+            total += from_plane[offset, rows, :].astype(full)
+        after_ref[rows, mine] = total.astype(half)
+
+    def swap(arriving):
+        columns = block_of(other if arriving else core, wide)
+        return remote(
+            after_ref.at[:, columns], after_ref.at[:, columns], sems.at[0, share],
+            sems.at[1, share], {"tp": other},
+        )
+
+    swap(False).start()
+    for offset in range(share):
+        pair(offset).wait_send()
+        if offset:
+            plane(offset).wait_send()
+    swap(False).wait_send()
+    swap(True).wait_recv()
+
+
+def middle_kernel(
+    share,
+    column,
+    left_ref,
+    weight_ref,
+    base_ref,
+    gain_ref,
+    after_ref,
+    rows_ref,
+    kept,
+    to_pair,
+    from_pair,
+    to_plane,
+    from_plane,
+    sems,
+    part,
+    plane_send,
+    plane_receive,
+    pair_send,
+    pair_receive,
+):
+    greet(share)
+    scratch = (kept, to_pair, from_pair, to_plane, from_plane, sems)
+    product_scatter(share, left_ref, weight_ref, column, base_ref, after_ref, scratch)
+    core = lax.axis_index("tp")
+    size = part.shape[0]
+
+    @pl.loop(0, size // 32)
+    def _(tile):
+        start = pl.multiple_of(core * size + tile * 32, 32)
+        values = after_ref[pl.ds(start, 32), :].astype(full)
+        inverse = lax.rsqrt(jnp.mean(values * values, axis=-1, keepdims=True) + epsilon)
+        part[block_of(tile, 32), :] = (values * inverse * gain_ref[...]).astype(half)
+
+    gather = Gather(share, part, rows_ref, plane_send, plane_receive, pair_send, pair_receive)
+    gather.start()
+    gather.finish()
+
+
+def last_kernel(
+    share,
+    left_ref,
+    weight_ref,
+    base_ref,
+    after_ref,
+    kept,
+    to_pair,
+    from_pair,
+    to_plane,
+    from_plane,
+    sems,
+):
+    greet(share)
+    scratch = (kept, to_pair, from_pair, to_plane, from_plane, sems)
+    product_scatter(share, left_ref, weight_ref, 0, base_ref, after_ref, scratch)
+
+
+def call(kernel, identity, outs, scratch, microseconds, *operands):
+    return pl.pallas_call(
+        kernel,
+        out_shape=outs,
+        in_specs=[VMEM] * len(operands),
+        out_specs=jax.tree.map(lambda _: VMEM, outs),
+        scratch_shapes=scratch,
+        compiler_params=pltpu.CompilerParams(collective_id=identity, has_side_effects=True),
+        cost_estimate=pl.CostEstimate(
+            flops=0, bytes_accessed=microseconds * 3_000_000, transcendentals=0
+        ),
+    )(*operands)
+
+
+def scatter_scratch(share, length, width):
+    slots = pltpu.VMEM((share, length, width // 2), half)
+    return [slots] * 5 + [pltpu.SemaphoreType.DMA((4, share + 1))]
+
+
+def gather_scratch(share):
+    return [pltpu.SemaphoreType.DMA((share,))] * 4
+
+
+def per_device_shared(
+    share,
+    tokens,
+    mixer_gain,
+    w_query,
+    w_key,
+    w_value,
+    gate_down,
+    gate_up,
+    decay_bias,
+    decay_shift,
+    head_gain,
+    w_out,
+    mlp_gain,
+    mlp_up,
+    mlp_down,
+):
+    depth = w_query.shape[0]
+    length, width = tokens.shape
+    place = lax.axis_index("share")
+    core = lax.axis_index("tp")
+    part = length // 2
+
+    def own_part(array, axis):
+        size = array.shape[axis] // share
+        return lax.dynamic_slice_in_dim(array, place * size, size, axis)
+
+    def spread(own):
+        return lax.all_gather(own, "band", axis=0, tiled=True)
+
+    wide_k = w_query.shape[1] // share
+    wide_v = w_value.shape[1] // share
+    wide = 2 * wide_k + wide_v
+    pairs = [pltpu.SemaphoreType.DMA((4, share))] * 2
+    own = call(
+        functools.partial(weights_kernel, share),
+        0,
+        jax.ShapeDtypeStruct((share * depth, wide + wide_v), half),
+        pairs,
+        12,
+        w_query,
+        w_key,
+        w_value,
+        w_out,
+    )
+    joined = spread(own)
+    mine = lax.dynamic_slice_in_dim(tokens, core * part, part, 0)
+    heads = decay_shift.shape[1]
+    shift_t = jnp.pad(decay_shift.T, ((0, -heads % 8), (0, 0)))
+    hidden_wide = mlp_up.shape[1] // share
+    weight_out = jax.ShapeDtypeStruct((share * depth, hidden_wide), half)
+    rows_shape = jax.ShapeDtypeStruct((share * length, width), half)
+    rows_all, shifts, up_own, down_own = call(
+        functools.partial(tokens_kernel, share),
+        1,
+        (
+            rows_shape,
+            jax.ShapeDtypeStruct((share,) + shift_t.shape, full),
+            weight_out,
+            weight_out,
+        ),
+        [pltpu.SemaphoreType.DMA((2, share))] * 2
+        + gather_scratch(share)
+        + [pltpu.SemaphoreType.DMA((share,))] * 2,
+        65,
+        rms_rows(mine, mixer_gain),
+        shift_t,
+        mlp_up,
+        mlp_down,
+    )
+    up_all = spread(up_own)
+    down_all = spread(down_own)
+    count = heads // share
+    shift = lax.dynamic_slice_in_dim(shifts, place * count, count, 1)
+    shift = shift.transpose(0, 2, 1).reshape(share * length, count)
+    gate_low = jnp.dot(rows_all, gate_down, preferred_element_type=full).astype(half)
+    sums = jnp.dot(rows_all, joined[:, :wide], preferred_element_type=full).astype(half)
+    query_sum, key_sum, value_sum = jnp.split(sums, (wide_k, 2 * wide_k), axis=1)
+    mixer_out = mix_heads(
+        query_sum,
+        key_sum,
+        value_sum,
+        gate_low,
+        own_part(gate_up, 1),
+        own_part(decay_bias, 0),
+        shift,
+        own_part(head_gain, 0),
+        share,
+    )
+    after_shape = jax.ShapeDtypeStruct((length, width), half)
+    after_mixer, rows_two = call(
+        functools.partial(middle_kernel, share, wide),
+        2,
+        (after_shape, rows_shape),
+        scatter_scratch(share, length, width)
+        + [pltpu.VMEM((part, width), half)]
+        + gather_scratch(share),
+        95,
+        mixer_out,
+        joined,
+        tokens,
+        mlp_gain.reshape(1, width),
+    )
+    pre = jnp.dot(rows_two, up_all, preferred_element_type=full)
+    hidden = jnp.square(jax.nn.relu(pre)).astype(half)
+    return call(
+        functools.partial(last_kernel, share),
+        3,
+        after_shape,
+        scatter_scratch(share, length, width),
+        55,
+        hidden,
+        down_all,
+        after_mixer,
     )
 
 
@@ -112,6 +591,7 @@
         decay_bias,
         decay_shift,
         head_gain,
+        1,
     )
     out_all = lax.all_gather(w_out, "fs", axis=0, tiled=True)
     mixer_term = times_transposed(mixer_out, out_all).astype(jnp.bfloat16).astype(jnp.float32)
@@ -131,25 +611,25 @@
 
 
 def solution(mesh):
-    return jax.shard_map(
-        per_device,
-        mesh=mesh,
-        in_specs=(
-            P("fs", None),
-            P(),
-            P("fs", "tp"),
-            P("fs", "tp"),
-            P("fs", "tp"),
-            P(),
-            P(None, "tp"),
-            P("tp"),
-            P("fs", "tp"),
-            P("tp"),
-            P("fs", "tp"),
-            P(),
-            P("fs", "tp"),
-            P("fs", "tp"),
-        ),
-        out_specs=P("fs", None),
-        check_vma=False,
-    )
+    bands, cores = mesh.devices.shape
+    fs = ("band", "share")
+    split = Mesh(mesh.devices.reshape(bands // SHARE, SHARE, cores), fs + ("tp",))
+
+    def layer(*arrays):
+        heads = arrays[8].shape[1] // cores
+        shared = cores == 2 and heads % SHARE == 0
+        axis = fs if shared else "fs"
+        body = functools.partial(per_device_shared, SHARE) if shared else per_device
+        row, both = P(axis, None), P(axis, "tp")
+        return jax.shard_map(
+            body,
+            mesh=split if shared else mesh,
+            in_specs=(
+                row, P(), both, both, both, P(), P(None, "tp"), P("tp"), both, P("tp"),
+                both, P(), both, both,
+            ),
+            out_specs=row,
+            check_vma=False,
+        )(*arrays)
+
+    return layer

time: 670 us -> 348 us (0.52)
  waiting for transfers between devices: 567 us -> 0.74 us
  Pallas kernels: 0 us -> 281 us
  matrix products: 57.2 us -> 39.6 us
  other arithmetic: 19.4 us -> 4.45 us
    all_gather x4 -> x3, waiting for transfers between devices: 526 us -> 0.02 us  [spread(): return lax.all_gather(own, 'band', axis=0, tiled=True)]
    pallas_call x0 -> x4, Pallas kernels: none -> 281 us  [call(): pl.pallas_call(kernel, out_shape=outs, in_specs=[VMEM] * len(operands), o...]
    psum x2 -> x0, waiting for transfers between devices: 38.5 us -> none  [the longest x1 19.6 us: per_device(): lax.psum(mlp_term.astype(jnp.bfloat16), 'tp').astype(jnp.float32)]
    dot_general x3 -> x2, matrix products: 38.1 us -> 22.3 us  [the longest x1 13.8 us: per_device_shared(): pre = jnp.dot(rows_two, up_all, preferred_element_type=full)]
    convert_element_type x3 -> x1, other arithmetic: 8.05 us -> 1.28 us  [rms_rows(): return (values * inverse * row_gain).astype(jnp.bfloat16)]
  transfers between devices with their start and end apart: 6 -> 3, of which waited for: 6 -> 0; matrix products, arithmetic and copies ran while one was open for 8% -> 14% of each run, Pallas kernels for 0% -> 57%
where the time goes in v1:
time: 348 us
  Pallas kernels  281 us (81%)
  matrix products  39.6 us (11%)
  between operations  13.4 us (4%)
  local copies, waits for them, and re-layouts  8.71 us (3%)
  other arithmetic  4.45 us (1%)
    pallas_call x4, Pallas kernels, call(): pl.pallas_call(kernel, out_shape=outs, in_specs=[VMEM] * len(operands), o...  281 us
    dot_general x1, matrix products, per_device_shared(): pre = jnp.dot(rows_two, up_all, preferred_element_type=full)  13.8 us
    dot_general x1, matrix products, per_device_shared(): jnp.dot(rows_all, joined[:, :wide], preferred_element_type=full)  8.5 us
  transfers between devices with their start and end apart: 3, of which 0 were waited for; matrix products, arithmetic and copies ran while one was open for 14% of the time, Pallas kernels for 57%

profile of v1, /device:TPU:0, one launch (start us, length us, event | category | flops | bytes accessed | tf_op | source)
XLA Modules:
  0.0 347.7 jit_solution(12453119494562328041)
XLA Ops:
  6.5 0.0 copy-start
  6.5 0.0 all-gather.4.cloned.1.call-start
  6.6 15.8 %shard_map.137 = bf16[512,768]{1,0:T(8,128)(2,1)} custom-call(bf16[128,512]{1,0:T(8,128)(2,1)} %q_ref.1, bf16[128,512]{1,0:T(8,128)(2,1)} %k_ref.1, bf16[128,1024]{1,0:T(8,128)(2,1)} %v_ref.1, bf16[128,1024]{1,0:T(8,128)(2,1)} %o_ref.1), custom_call_target="tpu_custom_call" | custom-call | bytes 36000000 | tf_op jit(solution)/shard_map/pallas_call | solution.py:423
  22.4 0.0 all-gather.4.cloned.1.call-update
  22.4 0.0 all-gather.6.cloned.1.call-start
  22.5 0.6 pad.4.shift_ref
  23.1 0.3 fusion.5
  23.4 1.3 fusion.7.part_ref
  24.7 82.9 %shard_map.136 = (bf16[2048,2048]{1,0:T(8,128)(2,1)}, f32[4,8,512]{2,1,0:T(8,128)}, bf16[512,1024]{1,0:T(8,128)(2,1)}, bf16[512,1024]{1,0:T(8,128)(2,1)}) custom-call(bf16[256,2048]{1,0:T(8,128)(2,1)} %fusion.7.part_ref, f32[8,512]{1,0:T(8,128)} %pad.4.shift_ref, bf16[128,4096]{1,0:T(8,128)(2,1)} %up_ref.1, bf16[128,4096]{1,0:T(8,128)(2,1)} %down_ref.1), custom_call_target="tpu_custom_call" | custom-call | bytes 195000000 | tf_op jit(solution)/shard_map/pallas_call | solution.py:423
  107.6 0.0 all-gather.6.cloned.1.call-update
  107.6 0.0 all-gather.8.cloned.1.call-start
  107.7 0.7 all-gather.8.cloned.1.call-update
  108.3 0.9 constant_dynamic-slice_fusion
  109.2 0.8 dynamic_slice.17
  110.0 0.0 copy-done
  110.0 5.3 %fusion.14 = f32[2048,128]{1,0:T(8,128)S(1)} fusion(bf16[2048,2048]{1,0:T(8,128)(2,1)} %get-tuple-element.11, bf16[2048,32]{0,1:T(8,128)(2,1)S(1)} %copy-done, f32[2048]{0:T(1024)S(1)} %bitcast.126, f32[128]{0:T(128)S(1)} %dynamic_slice.17, bf16[32,512]{1,0:T(8,128)(2,1)} %param.20, s32[]{:T(128)S(6)} %select_n.38), kind=kOutput, calls=%fused_computation.26 | convolution fusion | flops 288161792 | bytes 9585156 | tf_op jit(solution)/shard_map/dot_general | solution.py:36
  115.2 1.1 fusion.29
  116.4 0.1 bitcast_reduce_fusion
  116.4 0.7 broadcast_dynamic-update-slice_fusion.1
  117.2 0.1 copy.20
  117.3 0.1 copy.15
  117.4 0.8 dynamic_slice.19
  118.2 8.5 %convolution_convert_fusion = bf16[2048,512]{1,0:T(8,128)(2,1)S(1)} fusion(bf16[2048,2048]{1,0:T(8,128)(2,1)} %get-tuple-element.11, bf16[2048,768]{1,0:T(8,128)(2,1)} %all-gather.4.cloned.1.call-done.weight_ref), kind=kOutput, calls=%fused_computation.6 | convolution fusion | flops 4296015872 | bytes 12582912 | tf_op jit(solution)/shard_map/dot_general | solution.py:521
  126.7 0.1 convert_multiply_fusion.2
  126.8 0.1 split.14
  126.9 2.6 fusion.25
  129.5 1.3 fusion.18
  130.9 0.5 copy-done.5
  131.3 0.1 fusion.48
  131.5 0.2 convert_dynamic-update-slice_fusion.9
  131.7 0.1 convert_dynamic-update-slice_fusion.8
  131.8 0.2 convert_dynamic-update-slice_fusion.7
  132.0 0.1 convert_dynamic-update-slice_fusion.6
  132.2 0.9 convert_dynamic-update-slice_fusion.5
  133.1 0.1 convert_dynamic-update-slice_fusion.3
  133.3 0.2 fusion.49
  133.6 0.1 fusion.47
  133.7 0.0 copy-done.4
  133.8 2.2 fusion
  135.9 1.5 convolution_select_fusion
  137.4 3.4 multiply_reduce_fusion
  140.8 0.4 fusion.11
  141.1 1.0 copy.22
  142.2 116.7 %shard_map.138 = (bf16[512,2048]{1,0:T(8,128)(2,1)}, bf16[2048,2048]{1,0:T(8,128)(2,1)}) custom-call(bf16[2048,256]{1,0:T(8,128)(2,1)} %bitcast.123, bf16[2048,768]{1,0:T(8,128)(2,1)} %all-gather.4.cloned.1.call-done.weight_ref, bf16[512,2048]{1,0:T(8,128)(2,1)} %base_ref.1, f32[1,2048]{1,0:T(1,128)} %bitcast.124), custom_call_target="tpu_custom_call" | custom-call | bytes 285000000 | tf_op jit(solution)/shard_map/pallas_call | solution.py:423
  258.9 0.0 all-gather.6.cloned.1.call-done
  258.9 13.8 %multiply_convert_fusion.left_ref = bf16[2048,1024]{1,0:T(8,128)(2,1)} fusion(bf16[2048,2048]{1,0:T(8,128)(2,1)} %get-tuple-element.13, bf16[2048,1024]{1,0:T(8,128)(2,1)} %all-gather.6.cloned.1.call-done), kind=kOutput, calls=%fused_computation | convolution fusion | flops 8596226048 | bytes 16777216 | tf_op jit(solution)/shard_map/dot_general | solution.py:548
  272.7 65.3 %shard_map.139 = bf16[512,2048]{1,0:T(8,128)(2,1)} custom-call(bf16[2048,1024]{1,0:T(8,128)(2,1)} %multiply_convert_fusion.left_ref, bf16[2048,1024]{1,0:T(8,128)(2,1)} %all-gather.8.cloned.1.call-done.weight_ref, bf16[512,2048]{1,0:T(8,128)(2,1)} %get-tuple-element.16.base_ref), custom_call_target="tpu_custom_call" | custom-call | bytes 165000000 | tf_op jit(solution)/shard_map/pallas_call | solution.py:423
  338.0 3.2 copy.73
  (24 shorter events, 0.2 us)
Async XLA Ops:
  6.5 103.4 %copy-start = (bf16[2048,32]{0,1:T(8,128)(2,1)S(1)}, bf16[2048,32]{0,1:T(8,128)(2,1)}, u32[]{:S(2)}) copy-start(bf16[2048,32]{0,1:T(8,128)(2,1)} %param.19) | copy-start | bytes 393220
  6.5 15.9 %copy-start.7 = (f32[512,4]{0,1:T(4,128)S(1)}, f32[512,4]{0,1:T(4,128)}, u32[]{:S(2)}) copy-start(f32[512,4]{0,1:T(4,128)} %param.22) | copy-start | bytes 24580
  6.5 16.5 %copy-start.2 = (bf16[512,2048]{1,0:T(8,128)(2,1)S(1)}, bf16[512,2048]{1,0:T(8,128)(2,1)}, u32[]{:S(2)}) copy-start(bf16[512,2048]{1,0:T(8,128)(2,1)} %base_ref.1) | copy-start | bytes 6291460
  6.5 16.8 %copy-start.6 = (f32[2048]{0:T(1024)S(1)}, f32[2048]{0:T(1024)}, u32[]{:S(2)}) copy-start(f32[2048]{0:T(1024)} %param.15) | copy-start | bytes 24580
  6.5 111.7 %all-gather.4.cloned.1.call-start = ((), (), s32[]{:S(2)}) async-start(), calls=%async_computation | async-start | bytes 3932160 | tf_op jit(solution)/shard_map/all_gather | solution.py:473
  22.4 236.5 %all-gather.6.cloned.1.call-start = ((), (), s32[]{:S(2)}) async-start(), calls=%async_computation.1 | async-start | bytes 5242880 | tf_op jit(solution)/shard_map/all_gather | solution.py:473
  107.6 165.1 %all-gather.8.cloned.1.call-start = ((), (), s32[]{:S(2)}) async-start(), calls=%async_computation.2 | async-start | bytes 5242880 | tf_op jit(solution)/shard_map/all_gather | solution.py:473
  126.7 9.2 %copy-start.3 = (bf16[2048,512]{1,0:T(8,128)(2,1)}, bf16[2048,512]{1,0:T(8,128)(2,1)S(1)}, u32[]{:S(2)}) copy-start(bf16[2048,512]{1,0:T(8,128)(2,1)S(1)} %convolution_convert_fusion) | copy-start | bytes 6291460
  129.5 4.2 %copy-start.4 = (bf16[8,4,64,128]{3,2,1,0:T(8,128)(2,1)}, bf16[8,4,64,128]{3,2,1,0:T(8,128)(2,1)S(1)}, u32[]{:S(2)}) copy-start(bf16[8,4,64,128]{3,2,1,0:T(8,128)(2,1)S(1)} %get-tuple-element.36) | copy-start | bytes 1572868
  129.5 1.8 copy-start.5
  272.7 68.5 %copy-start.1 = (bf16[2048,32]{0,1:T(8,128)(2,1)S(1)}, bf16[2048,32]{0,1:T(8,128)(2,1)}, u32[]{:S(2)}) copy-start(bf16[2048,32]{0,1:T(8,128)(2,1)} %param.19) | copy-start | bytes 393220
Sparse Core Ops, SparseCore 0:
  22.5 63.8 all-gather.3
  107.7 80.6 all-gather.5
  190.0 79.2 all-gather.7

commit v2 on v1

--- a/solution.py
+++ b/solution.py
@@ -109,15 +109,27 @@
     return place
 
 
-def greet(share):
+def greet(share, along=False):
     place, core = lax.axis_index("share"), lax.axis_index("tp")
     barrier = pltpu.get_barrier_semaphore()
+    if along:
+        band, bands = lax.axis_index("band"), lax.axis_size("band")
+        for edge, step in ((0, -1), (bands - 1, 1)):
+
+            @pl.when(band != edge)
+            def _():
+                pl.semaphore_signal(
+                    barrier, inc=1, device_id={"band": band + step}, device_id_type=MESH
+                )
     for offset in range(1, share):
         pl.semaphore_signal(
             barrier, inc=1, device_id={"share": flip(place, offset)}, device_id_type=MESH
         )
     pl.semaphore_signal(barrier, inc=1, device_id={"tp": 1 - core}, device_id_type=MESH)
-    pl.semaphore_wait(barrier, share)
+    count = share
+    if along:
+        count = count + jnp.minimum(band, 1) + jnp.minimum(bands - 1 - band, 1)
+    pl.semaphore_wait(barrier, count)
 
 
 def remote(source, target, send, receive, device):
@@ -138,29 +150,29 @@
 def exchange_weights(share, weights, targets, send, receive):
     place = lax.axis_index("share")
     copies = []
-    for number, (weight, (target, column)) in enumerate(zip(weights, targets)):
+    for number, (weight, (target, first, column)) in enumerate(zip(weights, targets)):
         depth = weight.shape[0]
         size = weight.shape[1] // share
-        rows = block_of(place, depth)
+
+        def landing(owner):
+            start = pl.multiple_of(first + owner * depth, depth)
+            return target.at[pl.ds(start, depth), pl.ds(column, size)]
+
         for offset in range(share - 1, 0, -1):
             mate = flip(place, offset)
-            copy = remote(
-                weight.at[:, block_of(mate, size)],
-                target.at[rows, pl.ds(column, size)],
-                send.at[number, offset],
-                receive.at[number, offset],
-                {"share": mate},
-            )
+            copy, arrival = [
+                remote(
+                    weight.at[:, block_of(mate, size)],
+                    landing(owner),
+                    send.at[number, offset],
+                    receive.at[number, offset],
+                    {"share": mate},
+                )
+                for owner in (place, mate)
+            ]
             copy.start()
-            arrival = remote(
-                weight.at[:, block_of(mate, size)],
-                target.at[block_of(mate, depth), pl.ds(column, size)],
-                send.at[number, offset],
-                receive.at[number, offset],
-                {"share": mate},
-            )
             copies.append((copy, arrival))
-        target[rows, pl.ds(column, size)] = weight[:, block_of(place, size)]
+        landing(place)[...] = weight[:, block_of(place, size)]
     return copies
 
 
@@ -170,93 +182,156 @@
         arrival.wait_recv()
 
 
-def weights_kernel(share, q_ref, k_ref, v_ref, o_ref, out_ref, send, receive):
-    greet(share)
-    weights = (q_ref, k_ref, v_ref, o_ref)
-    targets, column = [], 0
-    for weight in weights:
-        targets.append((out_ref, column))
-        column += weight.shape[1] // share
-    finish(exchange_weights(share, weights, targets, send, receive))
+class Chain:
+    def __init__(self, target, send, receive):
+        self.target, self.send, self.receive = target, send, receive
+        self.band, self.bands = lax.axis_index("band"), lax.axis_size("band")
+        self.size = target.shape[0] // self.bands
+
+    def copy(self, way, step, block):
+        place = self.target.at[block_of(block, self.size)]
+        return remote(
+            place,
+            place,
+            self.send.at[way, step],
+            self.receive.at[way, step],
+            {"band": jnp.clip(self.band + 1 - 2 * way, 0, self.bands - 1)},
+        )
+
+    def each(self, step, arriving, action):
+        band, bands = self.band, self.bands
+        back = step + 1 if arriving else step
+        forth = 0 if arriving else 1
+        pl.when((band >= back) & (band + forth < bands))(
+            lambda: action(self.copy(0, step, band - back))
+        )
+        pl.when((band + back < bands) & (band >= forth))(
+            lambda: action(self.copy(1, step, band + back))
+        )
+
+    def start(self, step):
+        self.each(step, False, lambda copy: copy.start())
+
+    def arrive(self, step):
+        self.each(step, True, lambda copy: copy.wait_recv())
+
+    def finish(self):
+        for step in range(self.bands - 1):
+            self.each(step, False, lambda copy: copy.wait_send())
+
+
+X, Y, DIAGONAL = 1, 2, 3
+HOPS = ((X, 0), (X, 1), (Y, 0), (Y, 1), (X, 0), (Y, 1))
 
 
 class Gather:
-    def __init__(self, share, part, target, plane_send, plane_receive, pair_send, pair_receive):
-        self.share, self.part, self.target = share, part, target
-        self.plane_send, self.plane_receive = plane_send, plane_receive
-        self.pair_send, self.pair_receive = pair_send, pair_receive
+    def __init__(self, part, target, sems):
+        self.part, self.target, self.sems = part, target, sems
         self.place, self.core = lax.axis_index("share"), lax.axis_index("tp")
-
-    def rows(self, mate, core):
-        return block_of(mate * 2 + core, self.part.shape[0])
-
-    def plane(self, offset, arriving):
-        mate = flip(self.place, offset)
-        owner = mate if arriving else self.place
+        self.size = part.shape[0]
+
+    def rows(self, offset, core, piece=None):
+        first = (flip(self.place, offset) * 2 + core) * self.size
+        size = self.size
+        if piece is not None:
+            size = self.size // 2
+            first = first + piece * size
+        return pl.ds(pl.multiple_of(first, size), size)
+
+    def owner(self, slot, arriving):
+        way = HOPS[slot][0]
+        if slot < 4:
+            return way if arriving else 0
+        return DIAGONAL if arriving else X + Y - way
+
+    def plane(self, slot, arriving=False):
+        way, piece = HOPS[slot]
+        rows = self.target.at[self.rows(self.owner(slot, arriving), self.core, piece)]
+        source = rows
+        if slot < 4:
+            half_size = self.size // 2
+            source = self.part.at[pl.ds(piece * half_size, half_size)]
         return remote(
-            self.part,
-            self.target.at[self.rows(owner, self.core)],
-            self.plane_send.at[offset],
-            self.plane_receive.at[offset],
-            {"share": mate},
-        )
-
-    def pair(self, offset, arriving):
-        mate = flip(self.place, offset)
-        source = self.part if offset == 0 else self.target.at[self.rows(mate, self.core)]
+            source, rows, self.sems.at[0, slot], self.sems.at[1, slot],
+            {"share": flip(self.place, way)},
+        )
+
+    def pair(self, slot, arriving=False):
+        core = 1 - self.core if arriving else self.core
+        if slot == 6:
+            source, rows = self.part, self.target.at[self.rows(0, core)]
+        else:
+            offset = self.owner(slot, True)
+            rows = self.target.at[self.rows(offset, core, HOPS[slot][1])]
+            source = self.target.at[self.rows(offset, self.core, HOPS[slot][1])]
         return remote(
-            source,
-            self.target.at[self.rows(mate, 1 - self.core if arriving else self.core)],
-            self.pair_send.at[offset],
-            self.pair_receive.at[offset],
-            {"tp": 1 - self.core},
+            source, rows, self.sems.at[2, slot], self.sems.at[3, slot], {"tp": 1 - self.core}
         )
 
     def start(self):
-        for offset in range(self.share - 1, 0, -1):
-            self.plane(offset, False).start()
-        self.pair(0, False).start()
+        for slot in (2, 1, 0, 3):
+            self.plane(slot).start()
+        self.pair(6).start()
+        self.target[self.rows(0, self.core)] = self.part[...]
+
+    def arrive(self, *slots):
+        for slot in slots:
+            self.plane(slot, True).wait_recv()
+            if slot == 2:
+                self.plane(4).start()
+            if slot == 1:
+                self.plane(5).start()
+            self.pair(slot).start()
+
+    def from_pair(self, *slots):
+        for slot in slots:
+            self.pair(slot, True).wait_recv()
 
     def finish(self):
-        self.target[self.rows(self.place, self.core)] = self.part[...]
-        for offset in range(1, self.share):
-            self.plane(offset, True).wait_recv()
-            self.pair(offset, False).start()
-        for offset in range(self.share):
-            if offset:
-                self.plane(offset, False).wait_send()
-            self.pair(offset, False).wait_send()
-            self.pair(offset, True).wait_recv()
-
-
-def tokens_kernel(
+        for slot in range(7):
+            if slot < 6:
+                self.plane(slot).wait_send()
+            self.pair(slot).wait_send()
+
+
+def first_kernel(
     share,
     part_ref,
     shift_ref,
+    q_ref,
+    k_ref,
+    v_ref,
+    o_ref,
     up_ref,
     down_ref,
     rows_ref,
     shifts_ref,
+    joined_ref,
     up_out,
     down_out,
     send,
     receive,
-    plane_send,
-    plane_receive,
-    pair_send,
-    pair_receive,
+    chain_send,
+    chain_receive,
+    gather_sems,
     shift_send,
     shift_receive,
 ):
-    greet(share)
+    chain = Chain(joined_ref, chain_send, chain_receive)
+    greet(share, True)
     place = lax.axis_index("share")
-    gather = Gather(
-        share, part_ref, rows_ref, plane_send, plane_receive, pair_send, pair_receive
-    )
+    weights = (q_ref, k_ref, v_ref, o_ref)
+    targets, column = [], 0
+    for weight in weights:
+        targets.append((joined_ref, chain.band * chain.size, column))
+        column += weight.shape[1] // share
+    early = exchange_weights(share, weights, targets, send, receive)
+    gather = Gather(part_ref, rows_ref, gather_sems)
+    gather.start()
     shifts = []
     for offset in range(1, share):
         mate = flip(place, offset)
-        pair = [
+        copies = [
             remote(
                 shift_ref,
                 shifts_ref.at[owner],
@@ -266,23 +341,39 @@
             )
             for owner in (place, mate)
         ]
-        pair[0].start()
-        shifts.append(pair)
+        copies[0].start()
+        shifts.append(copies)
     shifts_ref[place] = shift_ref[...]
-    copies = exchange_weights(
-        share, (up_ref, down_ref), ((up_out, 0), (down_out, 0)), send, receive
-    )
-    gather.start()
+    late = exchange_weights(
+        share,
+        (up_ref, down_ref),
+        ((up_out, 0, 0), (down_out, 0, 0)),
+        send.at[pl.ds(4, 2)],
+        receive.at[pl.ds(4, 2)],
+    )
+    finish(early)
+    chain.start(0)
+    gather.arrive(2, 1)
+    last = chain.bands - 2
+    for step in range(last):
+        chain.arrive(step)
+        chain.start(step + 1)
+        if step == 0:
+            gather.arrive(0, 3)
+    gather.arrive(4, 5)
     finish(shifts)
+    gather.from_pair(*range(7))
     gather.finish()
-    finish(copies)
-
-
-def product_scatter(share, left_ref, weight_ref, column, base_ref, after_ref, scratch):
+    chain.arrive(last)
+    chain.finish()
+    finish(late)
+
+
+def product_scatter(share, left_ref, weight_ref, column, columns_of, base_ref, scratch, store):
     kept, to_pair, from_pair, to_plane, from_plane, sems = scratch
     place, core = lax.axis_index("share"), lax.axis_index("tp")
-    length, width = after_ref.shape
-    wide = width // 2
+    length, wide = kept.shape[1:]
+    narrow = wide // 2
     depth = left_ref.shape[1]
     other = 1 - core
 
@@ -292,19 +383,22 @@
             {"tp": other},
         )
 
-    def plane(offset):
+    routes = ((3, 0, X), (3, 1, Y), (X, 0, X), (Y, 1, Y), (X, 1, X), (Y, 0, Y))
+
+    def plane(slot):
+        offset, piece, way = routes[slot]
         return remote(
-            to_plane.at[offset], from_plane.at[offset], sems.at[2, offset], sems.at[3, offset],
-            {"share": flip(place, offset)},
+            to_plane.at[offset, piece], from_plane.at[slot], sems.at[2, slot],
+            sems.at[3, slot], {"share": flip(place, way)},
         )
 
     def multiply(offset):
         rows = block_of(flip(place, offset), length)
-        for columns, target in ((other, to_pair), (core, kept)):
+        for side, target in ((other, to_pair), (core, kept)):
 
             @pl.loop(0, wide // COLUMN_TILE)
             def _(tile):
-                start = pl.multiple_of(columns * wide + tile * COLUMN_TILE, COLUMN_TILE)
+                start = pl.multiple_of(side * wide + tile * COLUMN_TILE, COLUMN_TILE)
                 product = lax.dot_general(
                     left_ref[rows, :],
                     weight_ref[pl.ds(start, COLUMN_TILE), pl.ds(column, depth)],
@@ -313,7 +407,7 @@
                 )
                 target[offset, :, block_of(tile, COLUMN_TILE)] = product.astype(half)
 
-            if columns is other:
+            if side is other:
                 pair(offset).start()
 
     def combine(offset):
@@ -323,90 +417,86 @@
         def _(tile):
             rows = block_of(tile, ROW_TILE)
             total = kept[offset, rows, :].astype(full) + from_pair[offset, rows, :].astype(full)
-            to_plane[offset, rows, :] = total.astype(half)
-
-        if offset:
-            plane(offset).start()
-
-    order = list(range(share - 1, -1, -1))
-    multiply(order[0])
-    for number, offset in enumerate(order):
-        if number + 1 < share:
-            multiply(order[number + 1])
-        combine(offset)
-    for offset in order[:-1]:
-        plane(offset).wait_recv()
-    mine = block_of(core, wide)
+            total = total.astype(half)
+            to_plane[offset, 0, rows, :] = total[:, :narrow]
+            to_plane[offset, 1, rows, :] = total[:, narrow:]
+
+    def add(slot, arrived):
+        offset, piece, _ = routes[slot]
+        plane(arrived).wait_recv()
+
+        @pl.loop(0, length // ROW_TILE)
+        def _(tile):
+            rows = block_of(tile, ROW_TILE)
+            total = to_plane[offset, piece, rows, :].astype(full)
+            total += from_plane[arrived, rows, :].astype(full)
+            to_plane[offset, piece, rows, :] = total.astype(half)
+
+        plane(slot).start()
+
+    multiply(DIAGONAL)
+    multiply(X)
+    combine(DIAGONAL)
+    plane(0).start()
+    plane(1).start()
+    multiply(Y)
+    combine(X)
+    plane(2).start()
+    multiply(0)
+    combine(Y)
+    plane(3).start()
+    combine(0)
+    add(4, 1)
+    add(5, 0)
+    for slot in (2, 3, 4, 5):
+        plane(slot).wait_recv()
 
     @pl.loop(0, length // ROW_TILE)
     def _(tile):
         rows = block_of(tile, ROW_TILE)
-        total = base_ref[rows, mine].astype(full) + to_plane[0, rows, :].astype(full)
-        for offset in range(1, share):
-            total += from_plane[offset, rows, :].astype(full)
-        after_ref[rows, mine] = total.astype(half)
-
-    def swap(arriving):
-        columns = block_of(other if arriving else core, wide)
-        return remote(
-            after_ref.at[:, columns], after_ref.at[:, columns], sems.at[0, share],
-            sems.at[1, share], {"tp": other},
-        )
-
-    swap(False).start()
+        for piece, slots in ((0, (2, 5)), (1, (3, 4))):
+            total = to_plane[0, piece, rows, :].astype(full)
+            for slot in slots:
+                total += from_plane[slot, rows, :].astype(full)
+            for tile in range(narrow // COLUMN_TILE):
+                columns = columns_of(core, piece * (narrow // COLUMN_TILE) + tile)
+                value = total[:, tile * COLUMN_TILE : (tile + 1) * COLUMN_TILE]
+                value += base_ref[rows, columns].astype(full)
+                store(rows, core, piece * narrow + tile * COLUMN_TILE, value.astype(half))
+
     for offset in range(share):
         pair(offset).wait_send()
-        if offset:
-            plane(offset).wait_send()
-    swap(False).wait_send()
-    swap(True).wait_recv()
-
-
-def middle_kernel(
+    for slot in range(6):
+        plane(slot).wait_send()
+
+
+def swap_halves(ref, sems):
+    core = lax.axis_index("tp")
+    wide = ref.shape[1] // 2
+    copy, arrival = [
+        remote(
+            ref.at[:, block_of(side, wide)],
+            ref.at[:, block_of(side, wide)],
+            sems.at[0, 6],
+            sems.at[1, 6],
+            {"tp": 1 - core},
+        )
+        for side in (core, 1 - core)
+    ]
+    copy.start()
+    copy.wait_send()
+    arrival.wait_recv()
+
+
+def scatter_kernel(
     share,
     column,
+    step,
+    shift,
     left_ref,
     weight_ref,
     base_ref,
-    gain_ref,
-    after_ref,
-    rows_ref,
-    kept,
-    to_pair,
-    from_pair,
-    to_plane,
-    from_plane,
-    sems,
-    part,
-    plane_send,
-    plane_receive,
-    pair_send,
-    pair_receive,
-):
-    greet(share)
-    scratch = (kept, to_pair, from_pair, to_plane, from_plane, sems)
-    product_scatter(share, left_ref, weight_ref, column, base_ref, after_ref, scratch)
-    core = lax.axis_index("tp")
-    size = part.shape[0]
-
-    @pl.loop(0, size // 32)
-    def _(tile):
-        start = pl.multiple_of(core * size + tile * 32, 32)
-        values = after_ref[pl.ds(start, 32), :].astype(full)
-        inverse = lax.rsqrt(jnp.mean(values * values, axis=-1, keepdims=True) + epsilon)
-        part[block_of(tile, 32), :] = (values * inverse * gain_ref[...]).astype(half)
-
-    gather = Gather(share, part, rows_ref, plane_send, plane_receive, pair_send, pair_receive)
-    gather.start()
-    gather.finish()
-
-
-def last_kernel(
-    share,
-    left_ref,
-    weight_ref,
-    base_ref,
-    after_ref,
+    out_ref,
     kept,
     to_pair,
     from_pair,
@@ -415,8 +505,60 @@
     sems,
 ):
     greet(share)
+    wide = out_ref.shape[1] // 2
+
+    def columns_of(core, tile):
+        index = (core * (wide // COLUMN_TILE) + tile) * step + shift
+        return block_of(index, COLUMN_TILE)
+
+    def store(rows, core, start, value):
+        first = pl.multiple_of(core * wide + start, COLUMN_TILE)
+        out_ref[rows, pl.ds(first, COLUMN_TILE)] = value
+
     scratch = (kept, to_pair, from_pair, to_plane, from_plane, sems)
-    product_scatter(share, left_ref, weight_ref, 0, base_ref, after_ref, scratch)
+    product_scatter(share, left_ref, weight_ref, column, columns_of, base_ref, scratch, store)
+    swap_halves(out_ref, sems)
+
+
+def hidden_kernel(share, after_ref, gain_ref, up_ref, hidden_ref, rows_ref, part, sems):
+    greet(share)
+    core = lax.axis_index("tp")
+    size = part.shape[0]
+
+    @pl.loop(0, size // 32)
+    def _(tile):
+        start = pl.multiple_of(core * size + tile * 32, 32)
+        values = after_ref[pl.ds(start, 32), :].astype(full)
+        inverse = lax.rsqrt(jnp.mean(values * values, axis=-1, keepdims=True) + epsilon)
+        part[block_of(tile, 32), :] = (values * inverse * gain_ref[...]).astype(half)
+
+    gather = Gather(part, rows_ref, sems)
+    gather.start()
+
+    def product(offset, side):
+        rows = gather.rows(offset, side)
+
+        @pl.loop(0, hidden_ref.shape[1] // COLUMN_TILE)
+        def _(tile):
+            columns = block_of(tile, COLUMN_TILE)
+            pre = jnp.dot(rows_ref[rows, :], up_ref[:, columns], preferred_element_type=full)
+            hidden_ref[rows, columns] = jnp.square(jnp.maximum(pre, 0.0)).astype(half)
+
+    product(0, core)
+    gather.from_pair(6)
+    product(0, 1 - core)
+    gather.arrive(2, 1, 0, 3)
+    product(X, core)
+    gather.from_pair(0, 1)
+    product(X, 1 - core)
+    gather.arrive(4, 5)
+    product(Y, core)
+    gather.from_pair(2, 3)
+    product(Y, 1 - core)
+    product(DIAGONAL, core)
+    gather.from_pair(4, 5)
+    product(DIAGONAL, 1 - core)
+    gather.finish()
 
 
 def call(kernel, identity, outs, scratch, microseconds, *operands):
@@ -435,11 +577,9 @@
 
 def scatter_scratch(share, length, width):
     slots = pltpu.VMEM((share, length, width // 2), half)
-    return [slots] * 5 + [pltpu.SemaphoreType.DMA((4, share + 1))]
-
-
-def gather_scratch(share):
-    return [pltpu.SemaphoreType.DMA((share,))] * 4
+    quarter = pltpu.VMEM((share, 2, length, width // 4), half)
+    landed = pltpu.VMEM((6, length, width // 4), half)
+    return [slots] * 3 + [quarter, landed, pltpu.SemaphoreType.DMA((4, 7))]
 
 
 def per_device_shared(
@@ -463,6 +603,7 @@
     length, width = tokens.shape
     place = lax.axis_index("share")
     core = lax.axis_index("tp")
+    bands = lax.axis_size("band")
     part = length // 2
 
     def own_part(array, axis):
@@ -475,45 +616,37 @@
     wide_k = w_query.shape[1] // share
     wide_v = w_value.shape[1] // share
     wide = 2 * wide_k + wide_v
-    pairs = [pltpu.SemaphoreType.DMA((4, share))] * 2
-    own = call(
-        functools.partial(weights_kernel, share),
-        0,
-        jax.ShapeDtypeStruct((share * depth, wide + wide_v), half),
-        pairs,
-        12,
-        w_query,
-        w_key,
-        w_value,
-        w_out,
-    )
-    joined = spread(own)
     mine = lax.dynamic_slice_in_dim(tokens, core * part, part, 0)
     heads = decay_shift.shape[1]
     shift_t = jnp.pad(decay_shift.T, ((0, -heads % 8), (0, 0)))
     hidden_wide = mlp_up.shape[1] // share
     weight_out = jax.ShapeDtypeStruct((share * depth, hidden_wide), half)
     rows_shape = jax.ShapeDtypeStruct((share * length, width), half)
-    rows_all, shifts, up_own, down_own = call(
-        functools.partial(tokens_kernel, share),
-        1,
+    dma = pltpu.SemaphoreType.DMA
+    rows_all, shifts, joined, up_own, down_own = call(
+        functools.partial(first_kernel, share),
+        0,
         (
             rows_shape,
             jax.ShapeDtypeStruct((share,) + shift_t.shape, full),
+            jax.ShapeDtypeStruct((width, wide + wide_v), half),
             weight_out,
             weight_out,
         ),
-        [pltpu.SemaphoreType.DMA((2, share))] * 2
-        + gather_scratch(share)
-        + [pltpu.SemaphoreType.DMA((share,))] * 2,
+        [dma((6, share))] * 2 + [dma((2, bands))] * 2 + [dma((4, 7))] + [dma((share,))] * 2,
         65,
         rms_rows(mine, mixer_gain),
         shift_t,
+        w_query,
+        w_key,
+        w_value,
+        w_out,
         mlp_up,
         mlp_down,
     )
     up_all = spread(up_own)
-    down_all = spread(down_own)
+    split = share * depth // 2
+    down_halves = [spread(down_own[:split]), spread(down_own[split:])]
     count = heads // share
     shift = lax.dynamic_slice_in_dim(shifts, place * count, count, 1)
     shift = shift.transpose(0, 2, 1).reshape(share * length, count)
@@ -531,32 +664,44 @@
         own_part(head_gain, 0),
         share,
     )
-    after_shape = jax.ShapeDtypeStruct((length, width), half)
-    after_mixer, rows_two = call(
-        functools.partial(middle_kernel, share, wide),
-        2,
-        (after_shape, rows_shape),
-        scatter_scratch(share, length, width)
-        + [pltpu.VMEM((part, width), half)]
-        + gather_scratch(share),
-        95,
+    after_mixer = call(
+        functools.partial(scatter_kernel, share, wide, 1, 0),
+        1,
+        jax.ShapeDtypeStruct((length, width), half),
+        scatter_scratch(share, length, width),
+        45,
         mixer_out,
         joined,
         tokens,
+    )
+    hidden = call(
+        functools.partial(hidden_kernel, share),
+        2,
+        jax.ShapeDtypeStruct((share * length, hidden_wide), half),
+        [
+            pltpu.VMEM((share * length, width), half),
+            pltpu.VMEM((part, width), half),
+            dma((4, 7)),
+        ],
+        45,
+        after_mixer,
         mlp_gain.reshape(1, width),
-    )
-    pre = jnp.dot(rows_two, up_all, preferred_element_type=full)
-    hidden = jnp.square(jax.nn.relu(pre)).astype(half)
-    return call(
-        functools.partial(last_kernel, share),
-        3,
-        after_shape,
-        scatter_scratch(share, length, width),
-        55,
-        hidden,
-        down_all,
-        after_mixer,
-    )
+        up_all,
+    )
+    results = []
+    for number, down in enumerate(down_halves):
+        result = call(
+            functools.partial(scatter_kernel, share, 0, 2, number),
+            3 + number,
+            jax.ShapeDtypeStruct((length, width // 2), half),
+            scatter_scratch(share, length, width // 2),
+            25,
+            hidden,
+            down,
+            after_mixer,
+        )
+        results.append(result.reshape(length, -1, COLUMN_TILE))
+    return jnp.stack(results, axis=2).reshape(length, width)
 
 
 def per_device(
@@ -617,7 +762,8 @@
 
     def layer(*arrays):
         heads = arrays[8].shape[1] // cores
-        shared = cores == 2 and heads % SHARE == 0
+        block = arrays[2].shape[0] // bands * SHARE
+        shared = cores == 2 and heads % SHARE == 0 and block == 2 * COLUMN_TILE
         axis = fs if shared else "fs"
         body = functools.partial(per_device_shared, SHARE) if shared else per_device
         row, both = P(axis, None), P(axis, "tp")

time: 348 us -> 322 us (0.925)
  Pallas kernels: 281 us -> 241 us
  local copies, waits for them, and re-layouts: 8.71 us -> 20.9 us
  other arithmetic: 4.45 us -> 16.4 us
  matrix products: 39.6 us -> 28.6 us
    pallas_call x4 -> x5, Pallas kernels: 281 us -> 241 us  [call(): pl.pallas_call(kernel, out_shape=outs, in_specs=[VMEM] * len(operands), o...]
    dot_general x1 -> x0, matrix products: 13.8 us -> none  [per_device_shared(): pre = jnp.dot(rows_two, up_all, preferred_element_type=full)]
    another operation x0 -> x3, local copies, waits for them, and re-layouts: none -> 7.17 us  [per_device_shared(): return jnp.stack(results, axis=2).reshape(length, width)]
    unnamed x10, other arithmetic: 2.07 us -> 8.04 us
  transfers between devices with their start and end apart: 3 -> 3, of which waited for: 0 -> 0; matrix products, arithmetic and copies ran while one was open for 14% -> 15% of each run, Pallas kernels for 57% -> 41%
where the time goes in v2:
time: 322 us; the launch traced here: 321 us
  Pallas kernels  241 us (75%)
  matrix products  28.6 us (9%)
  local copies, waits for them, and re-layouts  20.9 us (6%)
  other arithmetic  16.4 us (5%)
  between operations  13.4 us (4%)
    pallas_call x5, Pallas kernels, call(): pl.pallas_call(kernel, out_shape=outs, in_specs=[VMEM] * len(operands), o...  241 us
    dot_general x1, matrix products, per_device_shared(): jnp.dot(rows_all, joined[:, :wide], preferred_element_type=full)  8.11 us
    unnamed x10, other arithmetic  8.04 us
    another operation x3, local copies, waits for them, and re-layouts, per_device_shared(): return jnp.stack(results, axis=2).reshape(length, width)  7.17 us
  transfers between devices with their start and end apart: 3, of which 0 were waited for; matrix products, arithmetic and copies ran while one was open for 15% of the time, Pallas kernels for 41%

profile of v2, /device:TPU:0, one launch (start us, length us, event | category | flops | bytes accessed | tf_op | source)
XLA Modules:
  0.0 321.5 jit_solution(14407706943240761943)
XLA Ops:
  6.5 1.6 fusion.5
  8.1 2.5 fusion.7.part_ref
  10.6 0.6 pad.4.shift_ref
  11.2 80.5 %shard_map.136 = (bf16[2048,2048]{1,0:T(8,128)(2,1)}, f32[4,8,512]{2,1,0:T(8,128)}, bf16[2048,768]{1,0:T(8,128)(2,1)}, bf16[512,1024]{1,0:T(8,128)(2,1)}, bf16[512,1024]{1,0:T(8,128)(2,1)}) custom-call(bf16[256,2048]{1,0:T(8,128)(2,1)} %fusion.7.part_ref, f32[8,512]{1,0:T(8,128)} %pad.4.shift_ref, bf16[128,512]{1,0:T(8,128)(2,1)} %q_ref.1, ...), custom_call_target="tpu_custom_call" | custom-call | bytes 195000000 | tf_op jit(solution)/shard_map/pallas_call | solution.py:565
  91.8 2.3 fusion.66
  94.1 0.7 all-gather.8.cloned.1.call-update
  94.8 0.9 constant_dynamic-slice_fusion
  95.7 0.8 dynamic_slice.17
  96.4 5.5 %fusion.14 = f32[2048,128]{1,0:T(8,128)S(1)} fusion(bf16[2048,2048]{1,0:T(8,128)(2,1)} %get-tuple-element.10, bf16[2048,32]{0,1:T(8,128)(2,1)S(1)} %copy-done, f32[2048]{0:T(1024)S(1)} %bitcast.123, f32[128]{0:T(128)S(1)} %dynamic_slice.17, bf16[32,512]{1,0:T(8,128)(2,1)} %param.20, s32[]{:T(128)S(6)} %select_n.38), kind=kOutput, calls=%fused_computation.26 | convolution fusion | flops 288161792 | bytes 9585156 | tf_op jit(solution)/shard_map/dot_general | solution.py:36
  101.9 1.1 fusion.29
  103.0 0.1 bitcast_reduce_fusion
  103.1 0.8 copy-done.4
  103.9 8.1 %convolution_convert_fusion = bf16[2048,512]{1,0:T(8,128)(2,1)S(1)} fusion(bf16[2048,2048]{1,0:T(8,128)(2,1)} %get-tuple-element.10, bf16[2048,768]{1,0:T(8,128)(2,1)S(1)} %copy-done.4), kind=kOutput, calls=%fused_computation.5 | convolution fusion | flops 4296015872 | bytes 12582912 | tf_op jit(solution)/shard_map/dot_general | solution.py:654
  112.0 0.1 convert_multiply_fusion.2
  112.3 3.0 fusion.25
  115.2 1.3 fusion.18
  116.6 0.1 fusion.48
  116.7 0.2 convert_dynamic-update-slice_fusion.9
  116.9 0.1 convert_dynamic-update-slice_fusion.8
  117.1 0.2 convert_dynamic-update-slice_fusion.7
  117.3 0.1 convert_dynamic-update-slice_fusion.6
  117.4 2.0 convert_dynamic-update-slice_fusion.5
  119.4 0.6 copy-done.2
  120.0 1.3 copy-done.8
  121.4 0.1 copy.20
  121.5 0.1 copy.15
  121.6 0.9 dynamic_slice.19
  122.5 0.7 convert_dynamic-update-slice_fusion.4
  123.3 1.9 convert_dynamic-update-slice_fusion.3
  125.1 0.7 convert_dynamic-update-slice_fusion.2
  125.9 2.2 fusion.49
  128.1 0.7 convert_dynamic-update-slice_fusion
  128.8 1.9 fusion.47
  130.7 0.7 broadcast_dynamic-update-slice_fusion
  131.4 3.8 %fusion = f32[8,4,64,256]{3,2,1,0:T(8,128)} fusion(bf16[8,4,128,256]{3,2,1,0:T(8,128)(2,1)} %broadcast_dynamic-update-slice_fusion, bf16[8,4,128,256]{3,2,1,0:T(8,128)(2,1)S(1)} %get-tuple-element.29, bf16[8,4,64,128]{3,2,1,0:T(8,128)(2,1)S(1)} %copy-done.7, bf16[8,4,64,128]{3,2,1,0:T(8,128)(2,1)S(1)} %copy-done.6), kind=kOutput, calls=%fused_computation | convolution fusion | flops 278921216 | bytes 7340032 | tf_op jit(solution)/shard_map/nhtd,nhdv->nhtv/dot_general | solution.py:81
  135.2 2.4 convolution_select_fusion
  137.7 3.4 %multiply_reduce_fusion = (f32[8,4,64]{2,1,0:T(4,128)S(1)}, f32[8,4,64,256]{3,2,1,0:T(8,128)S(1)}) fusion(f32[8,4,64,256]{3,2,1,0:T(8,128)} %fusion, bf16[4,8,64,1,256]{4,2,1,0,3:T(8,128)(2,1)S(1)} %bitcast.116, f32[8,4,64,64]{3,2,1,0:T(8,128)} %convolution_select_fusion, bf16[8,4,64,128]{3,2,1,0:T(8,128)(2,1)} %get-tuple-element.34, ...), kind=kOutput, calls=%fused_computation.16 | convolution fusion | flops 103675904 | bytes 8400896 | tf_op jit(solution)/shard_map/nhts,nhsv->nhtv/dot_general | solution.py:62
  141.0 0.3 fusion.11
  141.4 1.0 copy.22
  142.4 49.7 %shard_map.137.after_ref.base_ref = bf16[512,2048]{1,0:T(8,128)(2,1)} custom-call(bf16[2048,256]{1,0:T(8,128)(2,1)} %bitcast.121, bf16[2048,768]{1,0:T(8,128)(2,1)} %get-tuple-element.11.weight_ref, bf16[512,2048]{1,0:T(8,128)(2,1)} %base_ref.1), custom_call_target="tpu_custom_call" | custom-call | bytes 135000000 | tf_op jit(solution)/shard_map/pallas_call | solution.py:565
  192.1 50.4 %shard_map.138.left_ref = bf16[2048,1024]{1,0:T(8,128)(2,1)} custom-call(bf16[512,2048]{1,0:T(8,128)(2,1)} %shard_map.137.after_ref.base_ref, f32[1,2048]{1,0:T(1,128)} %bitcast.124, bf16[2048,1024]{1,0:T(8,128)(2,1)} %all-gather.4.cloned.1.call-done.up_ref), custom_call_target="tpu_custom_call" | custom-call | bytes 135000000 | tf_op jit(solution)/shard_map/pallas_call | solution.py:565
  242.6 30.4 %shard_map.139 = bf16[512,1024]{1,0:T(8,128)(2,1)} custom-call(bf16[2048,1024]{1,0:T(8,128)(2,1)} %shard_map.138.left_ref, bf16[1024,1024]{1,0:T(8,128)(2,1)} %all-gather.6.cloned.1.call-done.weight_ref, bf16[512,2048]{1,0:T(8,128)(2,1)} %shard_map.137.after_ref.base_ref), custom_call_target="tpu_custom_call" | custom-call | bytes 75000000 | tf_op jit(solution)/shard_map/pallas_call | solution.py:565
  273.1 1.9 stack_reshape.6
  274.9 30.4 %shard_map.140 = bf16[512,1024]{1,0:T(8,128)(2,1)} custom-call(bf16[2048,1024]{1,0:T(8,128)(2,1)} %shard_map.138.left_ref, bf16[1024,1024]{1,0:T(8,128)(2,1)} %all-gather.8.cloned.1.call-done.weight_ref, bf16[512,2048]{1,0:T(8,128)(2,1)} %shard_map.137.after_ref.base_ref), custom_call_target="tpu_custom_call" | custom-call | bytes 75000000 | tf_op jit(solution)/shard_map/pallas_call | solution.py:565
  305.3 2.1 stack_reshape.7
  307.4 1.5 pad_maximum_fusion
  308.9 3.2 %copy.23 = bf16[512,4,2,256]{3,2,1,0:T(2,128)(2,1)S(1)} copy(bf16[512,4,2,256]{3,1,0,2:T(4,128)(2,1)S(1)} %pad_maximum_fusion) | data formatting | bytes 4194304 | tf_op jit(solution)/shard_map/stack | solution.py:704
  312.2 2.8 reshape.100
  (35 shorter events, 0.4 us)
Async XLA Ops:
  6.5 89.9 %copy-start = (bf16[2048,32]{0,1:T(8,128)(2,1)S(1)}, bf16[2048,32]{0,1:T(8,128)(2,1)}, u32[]{:S(2)}) copy-start(bf16[2048,32]{0,1:T(8,128)(2,1)} %param.19) | copy-start | bytes 393220
  6.5 4.1 %copy-start.10 = (f32[512,4]{0,1:T(4,128)S(1)}, f32[512,4]{0,1:T(4,128)}, u32[]{:S(2)}) copy-start(f32[512,4]{0,1:T(4,128)} %param.22) | copy-start | bytes 24580
  6.5 185.6 %all-gather.4.cloned.1.call-start = ((), (), s32[]{:S(2)}) async-start(), calls=%async_computation | async-start | bytes 5242880 | tf_op jit(solution)/shard_map/all_gather | solution.py:614
  91.7 150.8 %all-gather.6.cloned.1.call-start = ((), (), s32[]{:S(2)}) async-start(), calls=%async_computation.1 | async-start | bytes 2621440 | tf_op jit(solution)/shard_map/all_gather | solution.py:614
  94.1 180.9 %all-gather.8.cloned.1.call-start = ((), (), s32[]{:S(2)}) async-start(), calls=%async_computation.2 | async-start | bytes 2621440 | tf_op jit(solution)/shard_map/all_gather | solution.py:614
  101.9 2.0 copy-start.4
  112.0 3.2 %copy-start.3 = (bf16[2048,512]{1,0:T(8,128)(2,1)}, bf16[2048,512]{1,0:T(8,128)(2,1)S(1)}, u32[]{:S(2)}) copy-start(bf16[2048,512]{1,0:T(8,128)(2,1)S(1)} %convolution_convert_fusion) | copy-start | bytes 6291460
  116.5 3.5 %copy-start.2 = (f32[8,4,256,256]{3,2,1,0:T(8,128)}, f32[8,4,256,256]{3,2,1,0:T(8,128)S(1)}, u32[]{:S(2)}) copy-start(f32[8,4,256,256]{3,2,1,0:T(8,128)S(1)} %fusion.18) | copy-start | bytes 25165828
  120.0 1.3 copy-start.8
  121.6 4.3 %copy-start.5 = (f32[1,4,128,256]{3,2,1,0:T(8,128)S(1)}, f32[1,4,128,256]{3,2,1,0:T(8,128)}, u32[]{:S(2)}) copy-start(f32[1,4,128,256]{3,2,1,0:T(8,128)} %get-tuple-element.16) | copy-start | bytes 1572868
  121.6 4.3 %copy-start.9 = (bf16[8,4,128,256]{3,2,1,0:T(8,128)(2,1)S(1)}, bf16[8,4,128,256]{3,2,1,0:T(8,128)(2,1)}, u32[]{:S(2)}) copy-start(bf16[8,4,128,256]{3,2,1,0:T(8,128)(2,1)} %copy-done.8) | copy-start | bytes 6291460
  125.9 5.5 %copy-start.6 = (bf16[8,4,64,128]{3,2,1,0:T(8,128)(2,1)S(1)}, bf16[8,4,64,128]{3,2,1,0:T(8,128)(2,1)}, u32[]{:S(2)}) copy-start(bf16[8,4,64,128]{3,2,1,0:T(8,128)(2,1)} %get-tuple-element.34) | copy-start | bytes 1572868
  125.9 5.5 %copy-start.7 = (bf16[8,4,64,128]{3,2,1,0:T(8,128)(2,1)S(1)}, bf16[8,4,64,128]{3,2,1,0:T(8,128)(2,1)}, u32[]{:S(2)}) copy-start(bf16[8,4,64,128]{3,2,1,0:T(8,128)(2,1)} %get-tuple-element.33) | copy-start | bytes 1572868
  308.9 6.1 %copy-start.1 = (bf16[2048,32]{0,1:T(8,128)(2,1)S(1)}, bf16[2048,32]{0,1:T(8,128)(2,1)}, u32[]{:S(2)}) copy-start(bf16[2048,32]{0,1:T(8,128)(2,1)} %param.19) | copy-start | bytes 393220
Sparse Core Ops, SparseCore 0:
  91.9 80.9 all-gather.3
  174.4 44.1 all-gather.5
  220.2 44.4 all-gather.7

commit v3 on v2

--- a/solution.py
+++ b/solution.py
@@ -125,7 +125,8 @@
         pl.semaphore_signal(
             barrier, inc=1, device_id={"share": flip(place, offset)}, device_id_type=MESH
         )
-    pl.semaphore_signal(barrier, inc=1, device_id={"tp": 1 - core}, device_id_type=MESH)
+    if share:
+        pl.semaphore_signal(barrier, inc=1, device_id={"tp": 1 - core}, device_id_type=MESH)
     count = share
     if along:
         count = count + jnp.minimum(band, 1) + jnp.minimum(bands - 1 - band, 1)
@@ -147,12 +148,15 @@
     return pl.ds(pl.multiple_of(index * size, size), size)
 
 
-def exchange_weights(share, weights, targets, send, receive):
+def exchange_weights(share, pieces, send, receive):
     place = lax.axis_index("share")
     copies = []
-    for number, (weight, (target, first, column)) in enumerate(zip(weights, targets)):
+    for number, (weight, skip, size, target, first, column) in enumerate(pieces):
         depth = weight.shape[0]
-        size = weight.shape[1] // share
+        stride = weight.shape[1] // share
+
+        def columns(mate):
+            return pl.ds(pl.multiple_of(mate * stride + skip, 128), size)
 
         def landing(owner):
             start = pl.multiple_of(first + owner * depth, depth)
@@ -162,7 +166,7 @@
             mate = flip(place, offset)
             copy, arrival = [
                 remote(
-                    weight.at[:, block_of(mate, size)],
+                    weight.at[:, columns(mate)],
                     landing(owner),
                     send.at[number, offset],
                     receive.at[number, offset],
@@ -172,7 +176,7 @@
             ]
             copy.start()
             copies.append((copy, arrival))
-        landing(place)[...] = weight[:, block_of(place, size)]
+        landing(place)[...] = weight[:, columns(place)]
     return copies
 
 
@@ -183,15 +187,15 @@
 
 
 class Chain:
-    def __init__(self, target, send, receive):
-        self.target, self.send, self.receive = target, send, receive
+    def __init__(self, target, send, receive, own=None):
+        self.target, self.send, self.receive, self.own = target, send, receive, own
         self.band, self.bands = lax.axis_index("band"), lax.axis_size("band")
         self.size = target.shape[0] // self.bands
 
     def copy(self, way, step, block):
         place = self.target.at[block_of(block, self.size)]
         return remote(
-            place,
+            self.own if step == 0 and self.own is not None else place,
             place,
             self.send.at[way, step],
             self.receive.at[way, step],
@@ -209,11 +213,18 @@
             lambda: action(self.copy(1, step, band + back))
         )
 
-    def start(self, step):
+    def start(self, step=0):
         self.each(step, False, lambda copy: copy.start())
+        if step == 0 and self.own is not None:
+            self.target[block_of(self.band, self.size)] = self.own[...]
 
     def arrive(self, step):
         self.each(step, True, lambda copy: copy.wait_recv())
+
+    def forward(self, step):
+        self.arrive(step)
+        if step < self.bands - 2:
+            self.start(step + 1)
 
     def finish(self):
         for step in range(self.bands - 1):
@@ -294,9 +305,22 @@
             self.pair(slot).wait_send()
 
 
+def norm_part(source_ref, gain_ref, part):
+    core = lax.axis_index("tp")
+    size = part.shape[0]
+
+    @pl.loop(0, size // 32)
+    def _(tile):
+        start = pl.multiple_of(core * size + tile * 32, 32)
+        values = source_ref[pl.ds(start, 32), :].astype(full)
+        inverse = lax.rsqrt(jnp.mean(values * values, axis=-1, keepdims=True) + epsilon)
+        part[block_of(tile, 32), :] = (values * inverse * gain_ref[...]).astype(half)
+
+
 def first_kernel(
     share,
-    part_ref,
+    tokens_ref,
+    gain_ref,
     shift_ref,
     q_ref,
     k_ref,
@@ -307,26 +331,32 @@
     rows_ref,
     shifts_ref,
     joined_ref,
-    up_out,
-    down_out,
+    up_one,
+    up_two,
+    up_three,
+    down_one,
+    down_two,
+    part,
     send,
     receive,
-    chain_send,
-    chain_receive,
+    chain_sems,
     gather_sems,
     shift_send,
     shift_receive,
 ):
-    chain = Chain(joined_ref, chain_send, chain_receive)
+    chain = Chain(joined_ref, chain_sems.at[0], chain_sems.at[1])
+    later = Chain(up_one, chain_sems.at[2], chain_sems.at[3])
     greet(share, True)
     place = lax.axis_index("share")
-    weights = (q_ref, k_ref, v_ref, o_ref)
-    targets, column = [], 0
-    for weight in weights:
-        targets.append((joined_ref, chain.band * chain.size, column))
-        column += weight.shape[1] // share
-    early = exchange_weights(share, weights, targets, send, receive)
-    gather = Gather(part_ref, rows_ref, gather_sems)
+    base = chain.band * chain.size
+    pieces, column = [], 0
+    for weight in (q_ref, k_ref, v_ref, o_ref):
+        size = weight.shape[1] // share
+        pieces.append((weight, 0, size, joined_ref, base, column))
+        column += size
+    early = exchange_weights(share, pieces, send, receive)
+    norm_part(tokens_ref, gain_ref, part)
+    gather = Gather(part, rows_ref, gather_sems)
     gather.start()
     shifts = []
     for offset in range(1, share):
@@ -344,37 +374,185 @@
         copies[0].start()
         shifts.append(copies)
     shifts_ref[place] = shift_ref[...]
+    pieces = []
+    for weight, targets in ((up_ref, (up_one, up_two, up_three)), (down_ref, (down_one, down_two))):
+        skip = 0
+        for target in targets:
+            size = target.shape[1]
+            pieces.append((weight, skip, size, target, base if target is up_one else 0, 0))
+            skip += size
     late = exchange_weights(
-        share,
-        (up_ref, down_ref),
-        ((up_out, 0, 0), (down_out, 0, 0)),
-        send.at[pl.ds(4, 2)],
-        receive.at[pl.ds(4, 2)],
+        share, pieces, send.at[pl.ds(4, 5)], receive.at[pl.ds(4, 5)]
     )
     finish(early)
-    chain.start(0)
+    chain.start()
     gather.arrive(2, 1)
-    last = chain.bands - 2
-    for step in range(last):
-        chain.arrive(step)
-        chain.start(step + 1)
+    steps = chain.bands - 1
+    for step in range(steps - 1):
+        chain.forward(step)
         if step == 0:
             gather.arrive(0, 3)
     gather.arrive(4, 5)
+    ready = share - 1
+    finish(late[:ready])
+    later.start()
     finish(shifts)
     gather.from_pair(*range(7))
     gather.finish()
-    chain.arrive(last)
+    chain.forward(steps - 1)
+    for step in range(steps):
+        later.forward(step)
+    finish(late[ready:])
     chain.finish()
-    finish(late)
-
-
-def product_scatter(share, left_ref, weight_ref, column, columns_of, base_ref, scratch, store):
+    later.finish()
+
+
+def attention_kernel(
+    rows_ref,
+    joined_ref,
+    gate_down_ref,
+    gate_up_ref,
+    bias_ref,
+    shift_ref,
+    gain_ref,
+    own_ref,
+    mixer_ref,
+    target_ref,
+    total_decay,
+    both_ref,
+    ahead_ref,
+    back_ref,
+    tails_ref,
+    values_ref,
+    added_ref,
+    states_ref,
+    result_ref,
+    chain_sems,
+):
+    chain = Chain(target_ref, chain_sems.at[0], chain_sems.at[1], own_ref)
+    greet(0, True)
+    chain.start()
+    length = both_ref.shape[0]
+    count = rows_ref.shape[0] // length
+
+    @pl.loop(0, count)
+    def _(sequence):
+        attend(
+            block_of(sequence, length), rows_ref, joined_ref, gate_down_ref, gate_up_ref,
+            bias_ref, shift_ref, gain_ref, mixer_ref, total_decay, both_ref, ahead_ref,
+            back_ref, tails_ref, values_ref, added_ref, states_ref, result_ref,
+        )
+        for step in range(chain.bands - 1):
+            after = min(step + 1, count - 1)
+
+            @pl.when(sequence == after)
+            def _():
+                chain.forward(step)
+
+    chain.finish()
+
+
+GROUP = 256
+
+
+def attend(
+    rows,
+    rows_ref,
+    joined_ref,
+    gate_down_ref,
+    gate_up_ref,
+    bias_ref,
+    shift_ref,
+    gain_ref,
+    mixer_ref,
+    total_decay,
+    both_ref,
+    ahead_ref,
+    back_ref,
+    tails_ref,
+    values_ref,
+    added_ref,
+    states_ref,
+    result_ref,
+):
+    length, head_k = ahead_ref.shape
+    head_v = values_ref.shape[1]
+    blocks = length // BLOCK_TOKENS
+
+    def dot(left, right, contract=((1,), (0,)), **options):
+        return lax.dot_general(
+            left, right, (contract, ((), ())), preferred_element_type=full, **options
+        )
+
+    row = lax.broadcasted_iota(jnp.int32, (GROUP, GROUP), 0)
+    column = lax.broadcasted_iota(jnp.int32, (GROUP, GROUP), 1)
+    same = row // BLOCK_TOKENS == column // BLOCK_TOKENS
+    lower = same & (row >= column)
+    upper = same & (row <= column)
+    lower_f = lower.astype(full)
+    upper_f = upper.astype(full)
+
+    for group in range(length // GROUP):
+        here = slice(group * GROUP, (group + 1) * GROUP)
+        these = pl.ds(pl.multiple_of(rows.start + group * GROUP, GROUP), GROUP)
+        row_block = rows_ref[these, :]
+        gate_low = dot(row_block, gate_down_ref[...]).astype(half)
+        gate_pre = dot(gate_low, gate_up_ref[...]) + bias_ref[...]
+        sigmoid = jnp.minimum(gate_pre, 0.0) - jnp.log1p(jnp.exp(-jnp.abs(gate_pre)))
+        log_decay = sigmoid / decay_temper + shift_ref[these, :]
+        ahead = dot(lower_f, log_decay, precision=highest)
+        back = dot(upper_f, log_decay, precision=highest)
+        per_block = log_decay.reshape(GROUP // BLOCK_TOKENS, BLOCK_TOKENS, head_k)
+        end = jnp.sum(per_block, axis=1, keepdims=True)
+        wide_end = jnp.broadcast_to(end, per_block.shape).reshape(GROUP, head_k)
+        for block in range(GROUP // BLOCK_TOKENS):
+            number = group * (GROUP // BLOCK_TOKENS) + block
+            total_decay[number] = jnp.exp(
+                jnp.broadcast_to(end[block], (8, head_k))
+            )
+        queries = dot(row_block, joined_ref[:, :head_k]).astype(half).astype(full)
+        queries = queries * head_k ** (-0.5)
+        keyed = dot(row_block, joined_ref[:, head_k : 2 * head_k]).astype(half).astype(full)
+        values = dot(row_block, joined_ref[:, 2 * head_k : 2 * head_k + head_v]).astype(half)
+        q_ahead = (queries * jnp.exp(ahead)).astype(half)
+        q_back = (queries * jnp.exp(back)).astype(half)
+        k_ahead = (keyed * jnp.exp(-ahead)).astype(half)
+        k_back = (keyed * jnp.exp(-back)).astype(half)
+        both_ref[here, :head_k] = q_ahead
+        both_ref[here, head_k:] = q_back
+        tails_ref[here, :head_k] = (keyed * jnp.exp(wide_end - ahead)).astype(half)
+        tails_ref[here, head_k:] = (keyed * jnp.exp(wide_end - back)).astype(half)
+        values_ref[here, :] = values
+        scores = jnp.where(lower, dot(q_ahead, k_ahead, ((1,), (1,))), 0.0)
+        scores += jnp.where(upper, dot(q_back, k_back, ((1,), (1,))), 0.0)
+        result_ref[here, :] = dot(scores.astype(half), values)
+    for block in range(blocks):
+        here = slice(block * BLOCK_TOKENS, (block + 1) * BLOCK_TOKENS)
+        added_ref[block] = dot(values_ref[here, :], tails_ref[here, :], ((0,), (0,)))
+    state = jnp.zeros((head_v, head_k), full)
+    for block in range(blocks):
+        states_ref[block, :, :head_k] = state.astype(half)
+        if block + 1 < blocks:
+            state = total_decay[block, :1] * state + added_ref[block, :, :head_k]
+    state = jnp.zeros((head_v, head_k), full)
+    for block in range(blocks - 1, -1, -1):
+        states_ref[block, :, head_k:] = state.astype(half)
+        if block:
+            state = total_decay[block, :1] * state + added_ref[block, :, head_k:]
+    for block in range(blocks):
+        here = slice(block * BLOCK_TOKENS, (block + 1) * BLOCK_TOKENS)
+        carried = dot(both_ref[here, :], states_ref[block], ((1,), (1,)))
+        outcome = result_ref[here, :] + carried
+        inverse = lax.rsqrt(jnp.mean(outcome * outcome, axis=-1, keepdims=True) + epsilon)
+        these = pl.ds(pl.multiple_of(rows.start + block * BLOCK_TOKENS, BLOCK_TOKENS), BLOCK_TOKENS)
+        mixer_ref[these, :] = (outcome * inverse * gain_ref[...]).astype(half)
+
+
+def product_scatter(share, left_ref, weights, base_ref, out_ref, scratch, between):
     kept, to_pair, from_pair, to_plane, from_plane, sems = scratch
     place, core = lax.axis_index("share"), lax.axis_index("tp")
     length, wide = kept.shape[1:]
     narrow = wide // 2
-    depth = left_ref.shape[1]
     other = 1 - core
 
     def pair(offset):
@@ -399,12 +577,15 @@
             @pl.loop(0, wide // COLUMN_TILE)
             def _(tile):
                 start = pl.multiple_of(side * wide + tile * COLUMN_TILE, COLUMN_TILE)
-                product = lax.dot_general(
-                    left_ref[rows, :],
-                    weight_ref[pl.ds(start, COLUMN_TILE), pl.ds(column, depth)],
-                    (((1,), (1,)), ((), ())),
-                    preferred_element_type=full,
-                )
+                product, first = 0.0, 0
+                for weight, column, depth in weights:
+                    product += lax.dot_general(
+                        left_ref[rows, pl.ds(first, depth)],
+                        weight[pl.ds(start, COLUMN_TILE), pl.ds(column, depth)],
+                        (((1,), (1,)), ((), ())),
+                        preferred_element_type=full,
+                    )
+                    first += depth
                 target[offset, :, block_of(tile, COLUMN_TILE)] = product.astype(half)
 
             if side is other:
@@ -448,7 +629,11 @@
     combine(0)
     add(4, 1)
     add(5, 0)
-    for slot in (2, 3, 4, 5):
+    between(0)
+    plane(2).wait_recv()
+    plane(3).wait_recv()
+    between(1)
+    for slot in (4, 5):
         plane(slot).wait_recv()
 
     @pl.loop(0, length // ROW_TILE)
@@ -458,12 +643,11 @@
             total = to_plane[0, piece, rows, :].astype(full)
             for slot in slots:
                 total += from_plane[slot, rows, :].astype(full)
-            for tile in range(narrow // COLUMN_TILE):
-                columns = columns_of(core, piece * (narrow // COLUMN_TILE) + tile)
-                value = total[:, tile * COLUMN_TILE : (tile + 1) * COLUMN_TILE]
-                value += base_ref[rows, columns].astype(full)
-                store(rows, core, piece * narrow + tile * COLUMN_TILE, value.astype(half))
-
+            columns = pl.ds(pl.multiple_of(core * wide + piece * narrow, narrow), narrow)
+            total += base_ref[rows, columns].astype(full)
+            out_ref[rows, columns] = total.astype(half)
+
+    swap_halves(out_ref, sems)
     for offset in range(share):
         pair(offset).wait_send()
     for slot in range(6):
@@ -488,13 +672,53 @@
     arrival.wait_recv()
 
 
-def scatter_kernel(
+def mixer_kernel(
     share,
     column,
-    step,
-    shift,
     left_ref,
     weight_ref,
+    base_ref,
+    up_own,
+    down_own,
+    out_ref,
+    up_target,
+    down_target,
+    kept,
+    to_pair,
+    from_pair,
+    to_plane,
+    from_plane,
+    sems,
+    chain_sems,
+):
+    greet(share, True)
+    chains = (
+        Chain(up_target, chain_sems.at[0], chain_sems.at[1], up_own),
+        Chain(down_target, chain_sems.at[2], chain_sems.at[3], down_own),
+    )
+    for chain in chains:
+        chain.start()
+    steps = chains[0].bands - 1
+
+    def between(step):
+        if step < steps:
+            for chain in chains:
+                chain.forward(step)
+
+    scratch = (kept, to_pair, from_pair, to_plane, from_plane, sems)
+    weights = ((weight_ref, column, left_ref.shape[1]),)
+    product_scatter(share, left_ref, weights, base_ref, out_ref, scratch, between)
+    for step in range(2, steps):
+        between(step)
+    for chain in chains:
+        chain.finish()
+
+
+def last_kernel(
+    share,
+    left_ref,
+    one_ref,
+    two_ref,
     base_ref,
     out_ref,
     kept,
@@ -505,53 +729,63 @@
     sems,
 ):
     greet(share)
-    wide = out_ref.shape[1] // 2
-
-    def columns_of(core, tile):
-        index = (core * (wide // COLUMN_TILE) + tile) * step + shift
-        return block_of(index, COLUMN_TILE)
-
-    def store(rows, core, start, value):
-        first = pl.multiple_of(core * wide + start, COLUMN_TILE)
-        out_ref[rows, pl.ds(first, COLUMN_TILE)] = value
-
     scratch = (kept, to_pair, from_pair, to_plane, from_plane, sems)
-    product_scatter(share, left_ref, weight_ref, column, columns_of, base_ref, scratch, store)
-    swap_halves(out_ref, sems)
-
-
-def hidden_kernel(share, after_ref, gain_ref, up_ref, hidden_ref, rows_ref, part, sems):
-    greet(share)
+    weights = tuple((ref, 0, ref.shape[1]) for ref in (one_ref, two_ref))
+    product_scatter(share, left_ref, weights, base_ref, out_ref, scratch, lambda step: None)
+
+
+def hidden_kernel(
+    share,
+    after_ref,
+    gain_ref,
+    up_one,
+    up_two,
+    up_three,
+    down_own,
+    hidden_ref,
+    down_target,
+    rows_ref,
+    part,
+    sems,
+    chain_sems,
+):
+    greet(share, True)
+    chain = Chain(down_target, chain_sems.at[0], chain_sems.at[1], down_own)
+    chain.start()
     core = lax.axis_index("tp")
-    size = part.shape[0]
-
-    @pl.loop(0, size // 32)
-    def _(tile):
-        start = pl.multiple_of(core * size + tile * 32, 32)
-        values = after_ref[pl.ds(start, 32), :].astype(full)
-        inverse = lax.rsqrt(jnp.mean(values * values, axis=-1, keepdims=True) + epsilon)
-        part[block_of(tile, 32), :] = (values * inverse * gain_ref[...]).astype(half)
-
+    norm_part(after_ref, gain_ref, part)
     gather = Gather(part, rows_ref, sems)
     gather.start()
 
     def product(offset, side):
         rows = gather.rows(offset, side)
-
-        @pl.loop(0, hidden_ref.shape[1] // COLUMN_TILE)
-        def _(tile):
-            columns = block_of(tile, COLUMN_TILE)
-            pre = jnp.dot(rows_ref[rows, :], up_ref[:, columns], preferred_element_type=full)
-            hidden_ref[rows, columns] = jnp.square(jnp.maximum(pre, 0.0)).astype(half)
-
+        first = 0
+        for up_ref in (up_one, up_two, up_three):
+            begin = first
+
+            @pl.loop(0, up_ref.shape[1] // COLUMN_TILE)
+            def _(tile):
+                columns = block_of(tile, COLUMN_TILE)
+                pre = jnp.dot(rows_ref[rows, :], up_ref[:, columns], preferred_element_type=full)
+                start = pl.multiple_of(begin + tile * COLUMN_TILE, COLUMN_TILE)
+                squared = jnp.square(jnp.maximum(pre, 0.0)).astype(half)
+                hidden_ref[rows, pl.ds(start, COLUMN_TILE)] = squared
+
+            first += up_ref.shape[1]
+
+    steps = chain.bands - 1
     product(0, core)
     gather.from_pair(6)
     product(0, 1 - core)
-    gather.arrive(2, 1, 0, 3)
+    gather.arrive(2, 1)
+    chain.forward(0)
+    gather.arrive(0, 3)
     product(X, core)
     gather.from_pair(0, 1)
     product(X, 1 - core)
     gather.arrive(4, 5)
+    for step in range(1, steps - 1):
+        chain.forward(step)
     product(Y, core)
     gather.from_pair(2, 3)
     product(Y, 1 - core)
@@ -559,6 +793,8 @@
     gather.from_pair(4, 5)
     product(DIAGONAL, 1 - core)
     gather.finish()
+    chain.arrive(steps - 1)
+    chain.finish()
 
 
 def call(kernel, identity, outs, scratch, microseconds, *operands):
@@ -610,32 +846,42 @@
         size = array.shape[axis] // share
         return lax.dynamic_slice_in_dim(array, place * size, size, axis)
 
-    def spread(own):
-        return lax.all_gather(own, "band", axis=0, tiled=True)
+    def weight(rows, columns):
+        return jax.ShapeDtypeStruct((rows, columns), half)
 
     wide_k = w_query.shape[1] // share
     wide_v = w_value.shape[1] // share
     wide = 2 * wide_k + wide_v
-    mine = lax.dynamic_slice_in_dim(tokens, core * part, part, 0)
     heads = decay_shift.shape[1]
     shift_t = jnp.pad(decay_shift.T, ((0, -heads % 8), (0, 0)))
     hidden_wide = mlp_up.shape[1] // share
-    weight_out = jax.ShapeDtypeStruct((share * depth, hidden_wide), half)
-    rows_shape = jax.ShapeDtypeStruct((share * length, width), half)
+    eighth = hidden_wide // 8
+    up_cuts = (2 * eighth, 2 * eighth, 4 * eighth)
+    down_cuts = (2 * eighth, 6 * eighth)
+    own_rows = share * depth
+    rows_shape = weight(share * length, width)
     dma = pltpu.SemaphoreType.DMA
-    rows_all, shifts, joined, up_own, down_own = call(
+    gain_row = mixer_gain.reshape(1, width)
+    rows_all, shifts, joined, up_one, up_two, up_three, down_one, down_two = call(
         functools.partial(first_kernel, share),
         0,
         (
             rows_shape,
             jax.ShapeDtypeStruct((share,) + shift_t.shape, full),
-            jax.ShapeDtypeStruct((width, wide + wide_v), half),
-            weight_out,
-            weight_out,
+            weight(width, wide + wide_v),
+            weight(width, up_cuts[0]),
+            weight(own_rows, up_cuts[1]),
+            weight(own_rows, up_cuts[2]),
+            weight(own_rows, down_cuts[0]),
+            weight(own_rows, down_cuts[1]),
         ),
-        [dma((6, share))] * 2 + [dma((2, bands))] * 2 + [dma((4, 7))] + [dma((share,))] * 2,
+        [pltpu.VMEM((part, width), half)]
+        + [dma((9, share))] * 2
+        + [dma((4, 2, bands)), dma((4, 7))]
+        + [dma((share,))] * 2,
         65,
-        rms_rows(mine, mixer_gain),
+        tokens,
+        gain_row,
         shift_t,
         w_query,
         w_key,
@@ -644,64 +890,76 @@
         mlp_up,
         mlp_down,
     )
-    up_all = spread(up_own)
-    split = share * depth // 2
-    down_halves = [spread(down_own[:split]), spread(down_own[split:])]
-    count = heads // share
-    shift = lax.dynamic_slice_in_dim(shifts, place * count, count, 1)
-    shift = shift.transpose(0, 2, 1).reshape(share * length, count)
-    gate_low = jnp.dot(rows_all, gate_down, preferred_element_type=full).astype(half)
-    sums = jnp.dot(rows_all, joined[:, :wide], preferred_element_type=full).astype(half)
-    query_sum, key_sum, value_sum = jnp.split(sums, (wide_k, 2 * wide_k), axis=1)
-    mixer_out = mix_heads(
-        query_sum,
-        key_sum,
-        value_sum,
-        gate_low,
+    shift = lax.dynamic_slice_in_dim(shifts, place, 1, 1)
+    shift = shift.reshape(share * length, 1)
+    blocks = length // BLOCK_TOKENS
+    mixer_out, up_two = call(
+        attention_kernel,
+        1,
+        (weight(share * length, wide_v), weight(width, up_cuts[1])),
+        [
+            pltpu.VMEM((blocks, 8, wide_k), full),
+            pltpu.VMEM((length, 2 * wide_k), half),
+            pltpu.VMEM((length, wide_k), half),
+            pltpu.VMEM((length, wide_k), half),
+            pltpu.VMEM((length, 2 * wide_k), half),
+            pltpu.VMEM((length, wide_v), half),
+            pltpu.VMEM((blocks, wide_v, 2 * wide_k), full),
+            pltpu.VMEM((blocks, wide_v, 2 * wide_k), half),
+            pltpu.VMEM((length, wide_v), full),
+            dma((2, 2, bands)),
+        ],
+        25,
+        rows_all,
+        joined,
+        gate_down,
         own_part(gate_up, 1),
-        own_part(decay_bias, 0),
+        own_part(decay_bias, 0).reshape(1, wide_k),
         shift,
-        own_part(head_gain, 0),
-        share,
-    )
-    after_mixer = call(
-        functools.partial(scatter_kernel, share, wide, 1, 0),
-        1,
-        jax.ShapeDtypeStruct((length, width), half),
-        scatter_scratch(share, length, width),
+        own_part(head_gain, 0).reshape(1, wide_v),
+        up_two,
+    )
+    after_mixer, up_three, down_one = call(
+        functools.partial(mixer_kernel, share, wide),
+        2,
+        (weight(length, width), weight(width, up_cuts[2]), weight(width, down_cuts[0])),
+        scatter_scratch(share, length, width) + [dma((4, 2, bands))],
         45,
         mixer_out,
         joined,
         tokens,
-    )
-    hidden = call(
+        up_three,
+        down_one,
+    )
+    hidden, down_two = call(
         functools.partial(hidden_kernel, share),
-        2,
-        jax.ShapeDtypeStruct((share * length, hidden_wide), half),
+        3,
+        (weight(share * length, hidden_wide), weight(width, down_cuts[1])),
         [
             pltpu.VMEM((share * length, width), half),
             pltpu.VMEM((part, width), half),
             dma((4, 7)),
+            dma((2, 2, bands)),
         ],
         45,
         after_mixer,
         mlp_gain.reshape(1, width),
-        up_all,
-    )
-    results = []
-    for number, down in enumerate(down_halves):
-        result = call(
-            functools.partial(scatter_kernel, share, 0, 2, number),
-            3 + number,
-            jax.ShapeDtypeStruct((length, width // 2), half),
-            scatter_scratch(share, length, width // 2),
-            25,
-            hidden,
-            down,
-            after_mixer,
-        )
-        results.append(result.reshape(length, -1, COLUMN_TILE))
-    return jnp.stack(results, axis=2).reshape(length, width)
+        up_one,
+        up_two,
+        up_three,
+        down_two,
+    )
+    return call(
+        functools.partial(last_kernel, share),
+        4,
+        weight(length, width),
+        scatter_scratch(share, length, width),
+        45,
+        hidden,
+        down_one,
+        down_two,
+        after_mixer,
+    )
 
 
 def per_device(
@@ -762,8 +1020,7 @@
 
     def layer(*arrays):
         heads = arrays[8].shape[1] // cores
-        block = arrays[2].shape[0] // bands * SHARE
-        shared = cores == 2 and heads % SHARE == 0 and block == 2 * COLUMN_TILE
+        shared = cores == 2 and heads == SHARE and bands > 2 * SHARE
         axis = fs if shared else "fs"
         body = functools.partial(per_device_shared, SHARE) if shared else per_device
         row, both = P(axis, None), P(axis, "tp")

time: 322 us -> 315 us (0.978)
  Pallas kernels: 241 us -> 303 us
  matrix products: 28.6 us -> 0 us
  other arithmetic: 16.4 us -> 0 us
  between operations: 13.4 us -> 0.05 us
  local copies, waits for them, and re-layouts: 20.9 us -> 11.8 us
    pallas_call x5, Pallas kernels: 241 us -> 303 us  [call(): pl.pallas_call(kernel, out_shape=outs, in_specs=[VMEM] * len(operands), o...]
    dot_general x8 -> x0, matrix products: 28.6 us -> none  [the longest x1 8.11 us: per_device_shared(): jnp.dot(rows_all, joined[:, :wide], preferred_element_type=full)]
    unnamed x10 -> x0, other arithmetic: 8.04 us -> none
    another operation x4 -> x0, local copies, waits for them, and re-layouts: 7.89 us -> none  [the longest x3 7.17 us: per_device_shared(): return jnp.stack(results, axis=2).reshape(length, width)]
    another operation x2 -> x0, other arithmetic: 3.67 us -> none  [the longest x1 2.19 us: mix_heads(): jnp.stack([s.astype(half) for s in before])]
  transfers between devices with their start and end apart: 3 -> 0, of which waited for: 0 -> 0; matrix products, arithmetic and copies ran while one was open for 15% -> 0% of each run, Pallas kernels for 41% -> 0%
where the time goes in v3:
time: 315 us
  Pallas kernels  303 us (96%)
  local copies, waits for them, and re-layouts  11.8 us (4%)
    pallas_call x5, Pallas kernels, call(): pl.pallas_call(kernel, out_shape=outs, in_specs=[VMEM] * len(operands), o...  303 us

profile of v3, /device:TPU:0, one launch (start us, length us, event | category | flops | bytes accessed | tf_op | source)
XLA Modules:
  0.0 314.6 jit_solution(6712548158763828805)
XLA Ops:
  0.0 0.0 copy-start
  0.0 1.3 dynamic-slice_bitcast_fusion.bias_ref
  1.3 1.3 dynamic_slice.15
  2.6 0.0 copy-done
  2.7 0.6 constant_dynamic-slice_fusion.1.gate_up_ref
  3.2 1.3 pad.4.shift_ref
  4.5 1.9 copy.16.gate_down_ref
  6.5 99.5 %shard_map.136 = (bf16[2048,2048]{1,0:T(8,128)(2,1)}, f32[4,8,512]{2,1,0:T(8,128)}, bf16[2048,768]{1,0:T(8,128)(2,1)}, bf16[2048,256]{1,0:T(8,128)(2,1)}, bf16[5...) custom-call(bf16[512,2048]{1,0:T(8,128)(2,1)} %base_ref.1, ...), custom_call_target="tpu_custom_call" | custom-call | bytes 195000000 | tf_op jit(solution)/shard_map/pallas_call | solution.py:801
  106.0 0.9 constant_dynamic-slice_fusion
  106.8 1.3 copy.17.shift_ref
  108.2 30.4 %shard_map.137 = (bf16[2048,256]{1,0:T(8,128)(2,1)}, bf16[2048,256]{1,0:T(8,128)(2,1)}) custom-call(bf16[2048,2048]{1,0:T(8,128)(2,1)} %get-tuple-element.20.rows_ref, bf16[2048,768]{1,0:T(8,128)(2,1)} %get-tuple-element.21.joined_ref.weight_ref, bf16[2048,32]{1,0:T(8,128)(2,1)} %copy.16.gate_down_ref, ...), custom_call_target="tpu_custom_call" | custom-call | bytes 75000000 | tf_op jit(solution)/shard_map/pallas_call | solution.py:801
  138.6 61.3 %shard_map.138 = (bf16[512,2048]{1,0:T(8,128)(2,1)}, bf16[2048,512]{1,0:T(8,128)(2,1)}, bf16[2048,256]{1,0:T(8,128)(2,1)}) custom-call(bf16[2048,256]{1,0:T(8,128)(2,1)} %get-tuple-element.24.left_ref, bf16[2048,768]{1,0:T(8,128)(2,1)} %get-tuple-element.21.joined_ref.weight_ref, bf16[512,2048]{1,0:T(8,128)(2,1)} %base_ref.1, ...), custom_call_target="tpu_custom_call" | custom-call | bytes 135000000 | tf_op jit(solution)/shard_map/pallas_call | solution.py:801
  199.8 59.8 %shard_map.139 = (bf16[2048,1024]{1,0:T(8,128)(2,1)}, bf16[2048,768]{1,0:T(8,128)(2,1)}) custom-call(bf16[512,2048]{1,0:T(8,128)(2,1)} %get-tuple-element.27.after_ref.base_ref, f32[1,2048]{1,0:T(1,128)} %bitcast.10, bf16[2048,256]{1,0:T(8,128)(2,1)} %get-tuple-element.28.up_one, bf16[2048,256]{1,0:T(8,128)(2,1)} %get-tuple-element.29.up_two, ...), custom_call_target="tpu_custom_call" | custom-call | bytes 135000000 | tf_op jit(solution)/shard_map/pallas_call | solution.py:801
  259.6 51.9 %shard_map.140 = bf16[512,2048]{1,0:T(8,128)(2,1)} custom-call(bf16[2048,1024]{1,0:T(8,128)(2,1)} %get-tuple-element.32.left_ref, bf16[2048,256]{1,0:T(8,128)(2,1)} %get-tuple-element.33.one_ref, bf16[2048,768]{1,0:T(8,128)(2,1)} %get-tuple-element.34.two_ref, bf16[512,2048]{1,0:T(8,128)(2,1)} %get-tuple-element.27.after_ref.base_ref), custom_call_target="tpu_custom_call" | custom-call | bytes 135000000 | tf_op jit(solution)/shard_map/pallas_call | solution.py:801
  311.5 3.2 %copy.19 = bf16[512,2048]{1,0:T(8,128)(2,1)} copy(bf16[512,2048]{1,0:T(8,128)(2,1)} %shard_map.140) | data formatting | bytes 4194304
Async XLA Ops:
  0.0 2.7 copy-start
